TPU v7x, 256 devices: a whole 4x4x8 slice. The times are simulated.
256 devices in a mesh: row: 32 (over z, x), col: 8 (over y, core).
Axes of the slice: x: 4, y: 4, z: 8, core: 2. Of those that a mesh axis runs over, the one named last changes fastest.
Arguments:
- tokens: bfloat16 [2, 32768, 2048], P(None, ('row', 'col')), may hold values from -6 to 6
- norm_gain: float32 [2048], replicated, may hold values from 0.1 to 1.9
- mix_weight: bfloat16 [2048, 1024], replicated, may hold values from -0.125 to 0.125
- gate_weight: bfloat16 [2048, 2048], replicated, may hold values from -0.125 to 0.125
- out_weight: bfloat16 [1024, 2048], replicated, may hold values from -0.1875 to 0.1875
Outputs:
- gated: bfloat16 [2, 32768, 2048], P(None, ('row', 'col'))
All inputs are finite; a program needn't handle non-finite values.
Results may differ from a plain program's by a relative error of at most 0.017.
Values may be sent and summed in bfloat16 or wider, within the bound.
No kernel may reach another device: no remote copies, remote signals or barrier semaphores. Data moves between devices by JAX's collectives and lax.ppermute only.
A program may use at most 128 MiB of HBM per device.

v0:
```python
import math

import jax
import jax.numpy as jnp
from jax import lax
from jax.sharding import Mesh
from jax.sharding import PartitionSpec as P

GROUP_DIM = 128
LEN1 = 128
ROW = ("row_0", "row_1")
ROW_COL = ("row_0", "row_1", "col")


def cut_along(value, dim, peers):
    before, after = (value.shape[:dim], value.shape[dim + 1 :])
    return jnp.moveaxis(value.reshape(*before, peers, -1, *after), dim, 0)


def laid_out(parts, dim):
    lengths = list(parts.shape[1:])
    lengths[dim] *= parts.shape[0]
    return jnp.moveaxis(parts, 0, dim).reshape(lengths)


def exchange_in_order(parts, axes, order):
    inside = parts.shape[1:]
    whole = parts.reshape(*(lax.axis_size(a) for a in axes), *inside)
    for k in order:
        whole = lax.all_to_all(whole, axes[k], k, k, tiled=True)
    return whole.reshape(-1, *inside)


def one_axis_at_a_time(value, axes, order, split_dim, concat_dim):
    parts = cut_along(value, split_dim, lax.axis_size(axes))
    return laid_out(exchange_in_order(parts, axes, order), concat_dim)


def tables(length, factor):
    indices = jnp.arange(length, dtype=jnp.int32)
    products = indices[:, None] * indices[None, :] % length
    angles = products.astype(jnp.float32) * (2.0 * math.pi / length)
    return (jnp.cos(angles) * factor, jnp.sin(angles) * factor)


def length_transform(values, first_span):
    item_count, span_total, column_count = values.shape
    second_span = span_total // first_span
    cos_first, sin_first = tables(first_span, span_total ** (-0.5))
    cos_second, sin_second = tables(second_span, 1.0)
    row_index = jnp.arange(first_span, dtype=jnp.int32)[:, None]
    col_index = jnp.arange(second_span, dtype=jnp.int32)[None, :]
    twist_angle = (row_index * col_index % span_total).astype(jnp.float32) * (
        2.0 * math.pi / span_total
    )
    twist_cos = jnp.cos(twist_angle)[None, :, :, None]
    twist_sin = jnp.sin(twist_angle)[None, :, :, None]
    arranged = values.reshape(item_count, first_span, second_span, column_count)
    part_real = jnp.einsum("ka,sabc->skbc", cos_first, arranged)
    part_imaginary = -jnp.einsum("ka,sabc->skbc", sin_first, arranged)
    turned_real = part_real * twist_cos + part_imaginary * twist_sin
    turned_imaginary = part_imaginary * twist_cos - part_real * twist_sin
    real_part = jnp.einsum("skbc,bm->smkc", turned_real, cos_second) + jnp.einsum(
        "skbc,bm->smkc", turned_imaginary, sin_second
    )
    imaginary = jnp.einsum("skbc,bm->smkc", turned_imaginary, cos_second) - jnp.einsum(
        "skbc,bm->smkc", turned_real, sin_second
    )
    return (
        real_part.reshape(item_count, span_total, column_count),
        imaginary.reshape(item_count, span_total, column_count),
    )


def local(tokens, norm_gain, mix_weight, gate_weight, out_weight):
    widened = tokens.astype(jnp.float32)
    inverse_rms = lax.rsqrt(jnp.mean(widened * widened, axis=-1, keepdims=True) + 1e-06)
    normed = (widened * inverse_rms * norm_gain).astype(jnp.bfloat16)
    mixed_in = jnp.dot(normed, mix_weight, preferred_element_type=jnp.float32).astype(jnp.bfloat16)
    half_dim = GROUP_DIM // 2
    cos_group, sin_group = tables(GROUP_DIM, GROUP_DIM ** (-0.5))
    left_table = cos_group[:, :half_dim]
    right_table = jnp.concatenate(
        [cos_group[:, half_dim : half_dim + 1], sin_group[:, 1:half_dim]], axis=1
    )
    incoming = lax.all_to_all(mixed_in, "col", split_axis=2, concat_axis=1, tiled=True)
    item_count = incoming.shape[0]
    row_count = incoming.shape[1]
    grouped = incoming.astype(jnp.float32).reshape(item_count, row_count, -1, GROUP_DIM)
    left_part = jnp.einsum("srgj,jk->srgk", grouped, left_table)
    right_part = jnp.einsum("srgj,jk->srgk", grouped, right_table)
    spectra = jnp.stack(
        [
            left_part.reshape(item_count, row_count, -1),
            right_part.reshape(item_count, row_count, -1),
        ],
        axis=2,
    )
    gate_value = jax.nn.sigmoid(jnp.dot(normed, gate_weight, preferred_element_type=jnp.float32))
    seq_count, block_rows = (spectra.shape[0], spectra.shape[1])
    pair_width = spectra.shape[3] // lax.axis_size(ROW)
    flat_index = lax.axis_index(ROW) * pair_width + jnp.arange(pair_width, dtype=jnp.int32)
    lone_pair = flat_index % half_dim == 0
    stacked = lax.all_to_all(
        spectra.astype(jnp.bfloat16), ROW, split_axis=3, concat_axis=1, tiled=True
    ).astype(spectra.dtype)
    width_here = stacked.shape[3]
    joined_in = jnp.concatenate([stacked[:, :, 0], stacked[:, :, 1]], axis=2)
    real_part, imaginary = length_transform(joined_in, LEN1)
    sum_pair = real_part[..., :width_here] + imaginary[..., width_here:]
    diff_pair = real_part[..., :width_here] - imaginary[..., width_here:]
    lower_half = jnp.where(lone_pair, real_part[..., :width_here], sum_pair).astype(jnp.bfloat16)
    upper_half = jnp.where(lone_pair, real_part[..., width_here:], diff_pair).astype(jnp.bfloat16)
    both_halves = jnp.stack([lower_half, upper_half], axis=2)
    returned = one_axis_at_a_time(both_halves, ROW, (0, 1), 1, 3)
    lower_half = returned[:, :, 0].reshape(seq_count, block_rows, -1, half_dim)
    upper_half = returned[:, :, 1].reshape(seq_count, block_rows, -1, half_dim)
    spectral = jnp.concatenate(
        [lower_half, upper_half[..., :1], jnp.flip(upper_half[..., 1:], axis=3)], axis=3
    )
    spectral = spectral.reshape(seq_count, block_rows, -1)
    spectral_rows = lax.all_to_all(spectral, "col", split_axis=1, concat_axis=2, tiled=True)
    mapped = jnp.dot(spectral_rows, out_weight, preferred_element_type=jnp.float32)
    return (gate_value * mapped).astype(jnp.bfloat16)


def solution(mesh):
    split = Mesh(mesh.devices.reshape(8, 4, mesh.shape["col"]), ("row_0", "row_1", "col"))
    return jax.shard_map(
        local,
        mesh=split,
        in_specs=(P(None, ROW_COL, None), P(), P(), P(), P()),
        out_specs=P(None, ROW_COL, None),
        check_vma=False,
    )
```

profile of v0, /device:TPU:1, one launch (start us, length us, event | category | flops | bytes accessed | tf_op | source)
XLA Modules:
  0.0 124.7 jit_solution(7634107121673975796)
XLA Ops:
  0.0 1.5 %fusion.24 = f32[2,128]{1,0:T(2,128)S(1)} fusion(bf16[2,128,2048]{2,1,0:T(8,128)(2,1)} %param.5), kind=kLoop, calls=%fused_computation.14 | loop fusion | flops 1572608 | bytes 1049600 | tf_op jit(solution)/shard_map/reduce_sum | solution.py:77
  1.5 3.8 %fusion.30 = bf16[2,128,1024]{2,1,0:T(8,128)(2,1)S(1)} fusion(bf16[2048,1024]{1,0:T(8,128)(2,1)} %param.7, bf16[2,128,2048]{2,1,0:T(8,128)(2,1)} %param.5, f32[2048]{0:T(1024)} %param.6, f32[2,128]{1,0:T(2,128)S(1)} %add_rsqrt_fusion), kind=kOutput, calls=%fused_computation.24 | convolution fusion | flops 1076101120 | bytes 5776384 | tf_op jit(solution)/shard_map/dot_general | solution.py:79
  5.4 1.1 copy.63
  6.5 6.6 %all-to-all-start = ((bf16[2,128,1024]{1,0,2:T(2,128)(2,1)}), bf16[2,128,1024]{1,0,2:T(2,128)(2,1)S(1)}, u32[]{:S(2)}, u32[]{:S(2)}) async-start(bf16[2,128,1024]{1,0,2:T(2,128)(2,1)} %copy.63), calls=%async_computation | async-start | bytes 1048576 | tf_op jit(solution)/shard_map/all_to_all | solution.py:86
  13.1 0.3 broadcast_multiply_fusion
  13.3 0.3 fusion.81
  13.6 8.8 %all-to-all-done = bf16[2,128,1024]{1,0,2:T(2,128)(2,1)S(1)} async-done(((bf16[2,128,1024]{1,0,2:T(2,128)(2,1)}), bf16[2,128,1024]{1,0,2:T(2,128)(2,1)S(1)}, u32[]{:S(2)}, u32[]{:S(2)}) %all-to-all-start) | async-done | bytes 524320 | tf_op jit(solution)/shard_map/all_to_all | solution.py:86
  22.4 0.5 copy.64
  22.9 0.3 fusion.33
  23.2 0.3 fusion.34
  23.6 1.3 %copy.65 = bf16[2,1024,2,64]{1,0,2,3:T(2,128)(2,1)} copy(bf16[2,1024,2,64]{1,3,0,2:T(8,128)(2,1)S(1)} %pad_maximum_fusion.4) | data formatting | bytes 1048576 | tf_op jit(solution)/shard_map/stack | solution.py:92
  24.9 10.5 %all-to-all-start.1 = ((bf16[2,1024,2,64]{1,0,2,3:T(2,128)(2,1)}), bf16[2,1024,2,64]{1,0,2,3:T(2,128)(2,1)S(1)}, u32[]{:S(2)}, u32[]{:S(2)}) async-start(bf16[2,1024,2,64]{1,0,2,3:T(2,128)(2,1)} %copy.65), calls=%async_computation.1 | async-start | bytes 1048576 | tf_op jit(solution)/shard_map/all_to_all | solution.py:104
  35.5 0.5 fusion.71
  36.0 14.9 %all-to-all-done.1 = bf16[2,1024,2,64]{1,0,2,3:T(2,128)(2,1)S(1)} async-done(((bf16[2,1024,2,64]{1,0,2,3:T(2,128)(2,1)}), bf16[2,1024,2,64]{1,0,2,3:T(2,128)(2,1)S(1)}, u32[]{:S(2)}, u32[]{:S(2)}) %all-to-all-start.1) | async-done | bytes 524320 | tf_op jit(solution)/shard_map/all_to_all | solution.py:104
  50.9 0.3 copy.100
  51.2 0.4 reshape.98
  51.6 0.4 fusion.116
  52.0 0.2 concatenate.16
  52.1 0.2 copy.67
  52.3 0.2 concatenate.17
  52.5 0.2 copy.68
  52.7 0.5 fusion.27
  53.2 0.5 convolution_bitcast_fusion
  53.7 1.3 %fusion.48 = f32[256,2,128,4]{2,0,3,1:T(8,128)S(1)} fusion(f32[2,128,256,4]{1,2,3,0:T(8,128)S(1)} %fusion.27, f32[2,128,256,4]{1,2,3,0:T(8,128)S(1)} %convolution_bitcast_fusion, f32[128,256]{0,1:T(8,128)S(1)} %get-tuple-element.9, f32[128,256]{0,1:T(8,128)S(1)} %get-tuple-element.10), kind=kOutput, calls=%fused_computation.52 | convolution fusion | flops 135921664 | bytes 3407872 | tf_op jit(solution)/shard_map/skbc,bm->smkc/dot_general | solution.py:63
  55.0 1.3 %fusion.46 = f32[256,2,128,4]{2,0,3,1:T(8,128)S(1)} fusion(f32[2,128,256,4]{1,2,3,0:T(8,128)S(1)} %convolution_bitcast_fusion, f32[2,128,256,4]{1,2,3,0:T(8,128)S(1)} %fusion.27, f32[128,256]{0,1:T(8,128)S(1)} %get-tuple-element.9, f32[128,256]{0,1:T(8,128)S(1)} %get-tuple-element.10), kind=kOutput, calls=%fused_computation.50 | convolution fusion | flops 135921664 | bytes 3407872 | tf_op jit(solution)/shard_map/skbc,bm->smkc/dot_general | solution.py:66
  56.3 2.3 %fusion.29 = f32[2,256,128,4]{2,1,3,0:T(8,128)} fusion(f32[256,2,128,4]{2,0,3,1:T(8,128)S(1)} %fusion.48, f32[2,128,256,4]{1,2,3,0:T(8,128)S(1)} %convolution_bitcast_fusion, f32[2,128,256,4]{1,2,3,0:T(8,128)S(1)} %fusion.27, f32[128,256]{0,1:T(8,128)S(1)} %get-tuple-element.9, f32[128,256]{0,1:T(8,128)S(1)} %get-tuple-element.10), kind=kOutput, calls=%fused_computation.23 | convolution fusion | flops 136183808 | bytes 4456448 | tf_op jit(solution)/shard_map/skbc,bm->smkc/dot_general | solution.py:63
  58.6 2.7 %reshape.92 = f32[2,32768,4]{1,2,0:T(4,128)} reshape(f32[2,256,128,4]{2,1,3,0:T(8,128)} %fusion.29) | data formatting | bytes 2097152 | tf_op jit(solution)/shard_map/reshape | solution.py:70
  61.3 2.3 %fusion.28 = f32[2,256,128,4]{2,1,3,0:T(8,128)} fusion(f32[256,2,128,4]{2,0,3,1:T(8,128)S(1)} %fusion.46, f32[2,128,256,4]{1,2,3,0:T(8,128)S(1)} %fusion.27, f32[2,128,256,4]{1,2,3,0:T(8,128)S(1)} %convolution_bitcast_fusion, f32[128,256]{0,1:T(8,128)S(1)} %get-tuple-element.9, f32[128,256]{0,1:T(8,128)S(1)} %get-tuple-element.10), kind=kOutput, calls=%fused_computation.21 | convolution fusion | flops 136183808 | bytes 4456448 | tf_op jit(solution)/shard_map/skbc,bm->smkc/dot_general | solution.py:66
  63.5 1.8 %reshape.93 = f32[2,32768,4]{1,2,0:T(4,128)S(1)} reshape(f32[2,256,128,4]{2,1,3,0:T(8,128)} %fusion.28) | data formatting | bytes 2097152 | tf_op jit(solution)/shard_map/reshape | solution.py:71
  65.3 0.8 fusion.37
  66.1 0.2 stack.14
  66.3 0.2 stack.15
  66.5 0.5 copy.75
  67.1 0.5 copy.76
  67.6 17.5 %all_to_all.52 = bf16[8,4,2,1024,2,2]{3,4,5,1,2,0:T(2,128)(2,1)S(1)} all-to-all(bf16[8,4,2,1024,2,2]{3,4,5,1,2,0:T(2,128)(2,1)S(1)} %copy.76), channel_id=1, replica_groups=mesh['row_0'=8,'row_1'=4,'col'=8] {'row_0'}, dimensions={0} | all-to-all | bytes 1048576 | tf_op jit(solution)/shard_map/all_to_all | solution.py:30
  85.1 0.4 copy.77
  85.5 10.9 %all_to_all.53 = bf16[8,4,2,1024,2,2]{3,4,5,0,2,1:T(2,128)(2,1)S(1)} all-to-all(bf16[8,4,2,1024,2,2]{3,4,5,0,2,1:T(2,128)(2,1)S(1)} %copy.77), channel_id=1, replica_groups=mesh['row_0'=8,'row_1'=4,'col'=8] {'row_1'}, dimensions={1} | all-to-all | bytes 1048576 | tf_op jit(solution)/shard_map/all_to_all | solution.py:30
  96.4 0.5 copy.78
  96.9 0.4 copy.79
  97.4 0.6 slice.60
  97.9 0.5 rev.4
  98.5 1.5 %pad_maximum_fusion.1 = bf16[2,1024,1,128]{1,2,3,0:T(2,128)(2,1)S(1)} fusion(bf16[2,1024,1,63]{1,2,3,0:T(2,128)(2,1)S(1)} %rev.4, bf16[2,1024,1,1]{1,2,3,0:T(2,128)(2,1)S(1)} %slice.59, bf16[2,1024,1,64]{1,2,3,0:T(2,128)(2,1)S(1)} %bitcast.112), kind=kLoop, calls=%fused_computation.30 | loop fusion | flops 524288 | bytes 1048576 | tf_op jit(solution)/shard_map/concatenate | solution.py:118
  100.0 0.9 copy.80
  100.9 1.3 %copy.81 = bf16[2,1024,128]{2,0,1:T(2,128)(2,1)} copy(bf16[2,1024,128]{2,1,0:T(8,128)(2,1)S(1)} %bitcast.113) | data formatting | bytes 1048576 | tf_op jit(solution)/shard_map/reshape | solution.py:121
  102.2 8.5 %all-to-all-start.4 = ((bf16[2,1024,128]{2,0,1:T(2,128)(2,1)}), bf16[2,1024,128]{2,0,1:T(2,128)(2,1)S(1)}, u32[]{:S(2)}, u32[]{:S(2)}) async-start(bf16[2,1024,128]{2,0,1:T(2,128)(2,1)} %copy.81), calls=%async_computation.4 | async-start | bytes 1048576 | tf_op jit(solution)/shard_map/all_to_all | solution.py:122
  110.8 6.2 %fusion.21 = f32[2,128,2048]{2,1,0:T(8,128)S(1)} fusion(bf16[2048,2048]{1,0:T(8,128)(2,1)} %param.8, bf16[2,128,2048]{2,1,0:T(8,128)(2,1)} %param.5, f32[2048]{0:T(1024)S(1)} %copy-done.1, f32[2,128]{1,0:T(2,128)S(1)} %add_rsqrt_fusion), kind=kOutput, calls=%fused_computation.13 | convolution fusion | flops 2151153664 | bytes 11543552 | tf_op jit(solution)/shard_map/dot_general | solution.py:99
  117.0 3.2 %all-to-all-done.4 = bf16[2,1024,128]{2,0,1:T(2,128)(2,1)S(1)} async-done(((bf16[2,1024,128]{2,0,1:T(2,128)(2,1)}), bf16[2,1024,128]{2,0,1:T(2,128)(2,1)S(1)}, u32[]{:S(2)}, u32[]{:S(2)}) %all-to-all-start.4) | async-done | bytes 524320 | tf_op jit(solution)/shard_map/all_to_all | solution.py:122
  120.2 4.5 %fusion.18 = bf16[2,128,2048]{2,1,0:T(8,128)(2,1)} fusion(f32[2,128,2048]{2,1,0:T(8,128)S(1)} %fusion.21, bf16[1024,2048]{1,0:T(8,128)(2,1)} %param.9, bf16[2,8,16,8,128]{4,3,2,1,0:T(8,128)(2,1)S(1)} %bitcast.119), kind=kOutput, calls=%fused_computation.12 | convolution fusion | flops 1074790400 | bytes 7864320 | tf_op jit(solution)/shard_map/dot_general | solution.py:123
  (12 shorter events, 0.2 us)
Async XLA Ops:
  6.5 16.0 %all-to-all-start = ((bf16[2,128,1024]{1,0,2:T(2,128)(2,1)}), bf16[2,128,1024]{1,0,2:T(2,128)(2,1)S(1)}, u32[]{:S(2)}, u32[]{:S(2)}) async-start(bf16[2,128,1024]{1,0,2:T(2,128)(2,1)} %copy.63), calls=%async_computation | async-start | bytes 1048576 | tf_op jit(solution)/shard_map/all_to_all | solution.py:86
  24.9 26.0 %all-to-all-start.1 = ((bf16[2,1024,2,64]{1,0,2,3:T(2,128)(2,1)}), bf16[2,1024,2,64]{1,0,2,3:T(2,128)(2,1)S(1)}, u32[]{:S(2)}, u32[]{:S(2)}) async-start(bf16[2,1024,2,64]{1,0,2,3:T(2,128)(2,1)} %copy.65), calls=%async_computation.1 | async-start | bytes 1048576 | tf_op jit(solution)/shard_map/all_to_all | solution.py:104
  63.5 1.8 %copy-start = (f32[2,32768,4]{1,2,0:T(4,128)S(1)}, f32[2,32768,4]{1,2,0:T(4,128)}, u32[]{:S(2)}) copy-start(f32[2,32768,4]{1,2,0:T(4,128)} %reshape.92) | copy-start | bytes 3145732
  100.0 10.8 %copy-start.1 = (f32[2048]{0:T(1024)S(1)}, f32[2048]{0:T(1024)}, u32[]{:S(2)}) copy-start(f32[2048]{0:T(1024)} %param.6) | copy-start | bytes 24580
  102.2 17.9 %all-to-all-start.4 = ((bf16[2,1024,128]{2,0,1:T(2,128)(2,1)}), bf16[2,1024,128]{2,0,1:T(2,128)(2,1)S(1)}, u32[]{:S(2)}, u32[]{:S(2)}) async-start(bf16[2,1024,128]{2,0,1:T(2,128)(2,1)} %copy.81), calls=%async_computation.4 | async-start | bytes 1048576 | tf_op jit(solution)/shard_map/all_to_all | solution.py:122
where the time goes:
time: 125 us
  blocking collectives  28.4 us (23%)
  waiting for transfers between devices  26.9 us (22%)
  starting transfers between devices  25.7 us (21%)
  matrix products  23.3 us (19%)
  local copies, waits for them, and re-layouts  15.2 us (12%)
  other arithmetic  4.97 us (4%)
    all_to_all x2, blocking collectives, exchange_in_order(): whole = lax.all_to_all(whole, axes[k], k, k, tiled=True)  28.4 us
    all_to_all x1, waiting for transfers between devices, local(): lax.all_to_all(spectra.astype(jnp.bfloat16), ROW, split_axis=3, concat_ax...  14.9 us
    all_to_all x1, starting transfers between devices, local(): lax.all_to_all(spectra.astype(jnp.bfloat16), ROW, split_axis=3, concat_ax...  10.5 us
    all_to_all x1, waiting for transfers between devices, local(): lax.all_to_all(mixed_in, 'col', split_axis=2, concat_axis=1, tiled=True)  8.82 us
    all_to_all x1, starting transfers between devices, local(): lax.all_to_all(spectral, 'col', split_axis=1, concat_axis=2, tiled=True)  8.54 us
    all_to_all x1, starting transfers between devices, local(): lax.all_to_all(mixed_in, 'col', split_axis=2, concat_axis=1, tiled=True)  6.6 us
    dot_general x1, matrix products, local(): jnp.dot(normed, gate_weight, preferred_element_type=jnp.float32)  6.2 us
    dot_general x1, matrix products, local(): jnp.dot(spectral_rows, out_weight, preferred_element_type=jnp.float32)  4.48 us
  transfers between devices with their start and end apart: 3, of which 3 were waited for; matrix products, arithmetic and copies ran while one was open for 6% of the time, Pallas kernels for 0%

commit v1 on v0

v1 whole, which is shorter than its diff:
```python
import jax
import jax.numpy as jnp
import numpy as np
from jax import lax
from jax.experimental import pallas as pl
from jax.experimental.pallas import tpu as pltpu
from jax.sharding import PartitionSpec as P

AXES = ("row", "col")
DEVICES = 256
SEQS = 2
BLOCK = 128
D = 2048
GROUPS = 8
GROUP_DIM = 128
FW = GROUPS * GROUP_DIM
LENGTH = 32768
PAIRS = 4
ROWS = 2 * PAIRS
NT = (((1,), (1,)), ((), ()))
F32, BF16 = jnp.float32, jnp.bfloat16


def group_table():
    table = np.zeros((GROUP_DIM, GROUP_DIM))
    j = np.arange(GROUP_DIM)
    for i in range(GROUP_DIM // ROWS):
        for p in range(PAIRS):
            k = PAIRS * i + p
            table[i * ROWS + p] = np.cos(2 * np.pi * j * k / GROUP_DIM)
            table[i * ROWS + PAIRS + p] = np.sin(2 * np.pi * j * k / GROUP_DIM)
    table[PAIRS] = np.cos(np.pi * j)
    return table / 8


def channel_order():
    order = np.zeros((GROUP_DIM, GROUP_DIM))
    for i in range(GROUP_DIM // ROWS):
        for p in range(PAIRS):
            k = PAIRS * i + p
            order[i * ROWS + p, k] = 1
            order[i * ROWS + PAIRS + p, (GROUP_DIM - k) if k else GROUP_DIM // 2] = 1
    return order


def first_table():
    m, d = np.arange(DEVICES)[:, None], np.arange(DEVICES)[None, :]
    angle = 2 * np.pi * (m * d % DEVICES) / DEVICES
    return np.concatenate([np.cos(angle), np.sin(angle)], axis=0) / 16


def twiddle():
    m, l = np.arange(DEVICES)[:, None], np.arange(BLOCK)[None, :]
    angle = 2 * np.pi * (m * l) / LENGTH
    return np.stack([np.cos(angle), np.sin(angle)])


def second_table():
    m, l = np.arange(BLOCK)[:, None], np.arange(BLOCK)[None, :]
    angle = 2 * np.pi * (m * l % BLOCK) / BLOCK
    return np.concatenate([np.cos(angle), -np.sin(angle)], axis=1) / 16


def enter_body(tokens, gain, weight, table, out, normed):
    @pl.when(pl.program_id(0) == 0)
    def _():
        for s in range(SEQS):

            def rows(i, _):
                at = pl.ds(pl.multiple_of(i * 16, 16), 16)
                t = tokens[s, at, :].astype(F32)
                inv = lax.rsqrt(jnp.mean(t * t, axis=-1, keepdims=True) + 1e-6)
                to = pl.ds(pl.multiple_of(s * BLOCK + i * 16, 16), 16)
                normed[to, :] = (t * inv * gain[...]).astype(BF16)
                return 0

            lax.fori_loop(0, BLOCK // 16, rows, 0)

    mixed = jnp.dot(normed[...], weight[...], preferred_element_type=F32).astype(BF16)
    for q in range(mixed.shape[1] // GROUP_DIM):
        at = slice(q * GROUP_DIM, (q + 1) * GROUP_DIM)
        turned = lax.dot_general(table[...], mixed[:, at], NT, preferred_element_type=F32)
        for s in range(SEQS):
            out[s, at, :] = turned[:, s * BLOCK : (s + 1) * BLOCK].astype(BF16)


def enter(tokens, gain, weight):
    steps = 4
    wide = FW // steps
    return pl.pallas_call(
        enter_body,
        grid=(steps,),
        in_specs=[
            pl.BlockSpec((SEQS, BLOCK, D), lambda j: (0, 0, 0)),
            pl.BlockSpec((1, D), lambda j: (0, 0)),
            pl.BlockSpec((D, wide), lambda j: (0, j)),
            pl.BlockSpec((GROUP_DIM, GROUP_DIM), lambda j: (0, 0)),
        ],
        out_specs=[
            pl.BlockSpec((SEQS, wide, BLOCK), lambda j: (0, j, 0)),
            pl.BlockSpec((SEQS * BLOCK, D), lambda j: (0, 0)),
        ],
        out_shape=[
            jax.ShapeDtypeStruct((SEQS, FW, BLOCK), BF16),
            jax.ShapeDtypeStruct((SEQS * BLOCK, D), BF16),
        ],
        name="enter",
    )(tokens, gain.reshape(1, D), weight, jnp.asarray(group_table(), BF16))


def length_body(lone, x, first, twist, second, y, wide_in, wide_out):
    wide_in[...] = x[...].astype(F32)
    own = lone[0]
    cos, sin = twist[0], twist[1]
    for p in range(PAIRS):
        pair = jnp.concatenate(
            [
                wide_in[pl.ds(p, DEVICES, stride=ROWS), :].astype(BF16),
                wide_in[pl.ds(PAIRS + p, DEVICES, stride=ROWS), :].astype(BF16),
            ],
            axis=1,
        )
        both = jnp.dot(first[...], pair, preferred_element_type=F32)
        parts = []
        for q in range(2):
            real = both[:DEVICES, q * BLOCK : (q + 1) * BLOCK]
            imag = both[DEVICES:, q * BLOCK : (q + 1) * BLOCK]
            if q == 0:
                c, s = cos, sin
            elif p == 0:
                c, s = own * cos + (1 - own) * sin, own * sin - (1 - own) * cos
            else:
                c, s = sin, -cos
            turned = jnp.concatenate(
                [(real * c - imag * s).astype(BF16), (real * s + imag * c).astype(BF16)], axis=1
            )
            parts.append(lax.dot_general(second[...], turned, NT, preferred_element_type=F32))
        if p == 0:
            low, high = parts[0] - (1 - own) * parts[1], (1 - own) * parts[0] + parts[1]
        else:
            low, high = parts[0] - parts[1], parts[0] + parts[1]
        for h in range(2):
            at = slice(h * BLOCK, (h + 1) * BLOCK)
            wide_out[pl.ds(h * ROWS + p, BLOCK, stride=2 * ROWS), :] = low[:, at]
            wide_out[pl.ds(h * ROWS + PAIRS + p, BLOCK, stride=2 * ROWS), :] = high[:, at]
    y[...] = wide_out[...].astype(BF16)


def length_transform(x, lone):
    vmem = pl.BlockSpec(memory_space=pltpu.VMEM)
    rows = DEVICES * ROWS
    return pl.pallas_call(
        length_body,
        in_specs=[pl.BlockSpec(memory_space=pltpu.SMEM), vmem, vmem, vmem, vmem],
        out_specs=vmem,
        out_shape=jax.ShapeDtypeStruct((rows, BLOCK), BF16),
        scratch_shapes=[pltpu.VMEM((rows, BLOCK), F32), pltpu.VMEM((rows, BLOCK), F32)],
        name="length",
    )(
        lone,
        x,
        jnp.asarray(first_table(), BF16),
        jnp.asarray(twiddle(), F32),
        jnp.asarray(second_table(), BF16),
    )


def gate_body(normed, weight, out):
    logits = jnp.dot(normed[...], weight[...], preferred_element_type=F32)
    out[...] = jax.nn.sigmoid(logits)


def gate(normed, weight):
    steps = 8
    wide = D // steps
    return pl.pallas_call(
        gate_body,
        grid=(steps,),
        in_specs=[
            pl.BlockSpec((SEQS * BLOCK, D), lambda j: (0, 0)),
            pl.BlockSpec((D, wide), lambda j: (0, j)),
        ],
        out_specs=pl.BlockSpec((SEQS * BLOCK, wide), lambda j: (0, j)),
        out_shape=jax.ShapeDtypeStruct((SEQS * BLOCK, D), F32),
        cost_estimate=pl.CostEstimate(
            flops=2 * SEQS * BLOCK * D * D, transcendentals=SEQS * BLOCK * D, bytes_accessed=2 * D * D
        ),
        name="gate",
    )(normed, weight)


def leave_body(z, order, eye, weight, gates, out, spectral):
    @pl.when(pl.program_id(0) == 0)
    def _():
        for s in range(SEQS):
            for g in range(GROUPS):
                rows = z[pl.ds(s * FW + g * GROUP_DIM, GROUP_DIM), :]
                turned = lax.dot_general(eye[...], rows, NT, preferred_element_type=F32)
                placed = jnp.dot(turned.astype(BF16), order[...], preferred_element_type=F32)
                spectral[s * BLOCK : (s + 1) * BLOCK, g * GROUP_DIM : (g + 1) * GROUP_DIM] = (
                    placed.astype(BF16)
                )

    mapped = jnp.dot(spectral[...], weight[...], preferred_element_type=F32)
    gated = (gates[...] * mapped).astype(BF16)
    for s in range(SEQS):
        out[s] = gated[s * BLOCK : (s + 1) * BLOCK]


def leave(z, gates, weight):
    steps = 4
    wide = D // steps
    square = pl.BlockSpec((GROUP_DIM, GROUP_DIM), lambda j: (0, 0))
    return pl.pallas_call(
        leave_body,
        grid=(steps,),
        in_specs=[
            pl.BlockSpec((SEQS * FW, BLOCK), lambda j: (0, 0)),
            square,
            square,
            pl.BlockSpec((FW, wide), lambda j: (0, j)),
            pl.BlockSpec((SEQS * BLOCK, wide), lambda j: (0, j)),
        ],
        out_specs=pl.BlockSpec((SEQS, BLOCK, wide), lambda j: (0, 0, j)),
        out_shape=jax.ShapeDtypeStruct((SEQS, BLOCK, D), BF16),
        scratch_shapes=[pltpu.VMEM((SEQS * BLOCK, FW), BF16)],
        name="leave",
    )(z, jnp.asarray(channel_order(), BF16), jnp.asarray(np.eye(GROUP_DIM), BF16), weight, gates)


def exchange(x):
    return lax.all_to_all(x.reshape(DEVICES, ROWS, BLOCK), AXES, 0, 0, tiled=True).reshape(
        DEVICES * ROWS, BLOCK
    )


def local(tokens, norm_gain, mix_weight, gate_weight, out_weight):
    spectra, normed = enter(tokens, norm_gain, mix_weight)
    lone = (lax.axis_index(AXES) % (GROUP_DIM // ROWS) == 0).astype(F32).reshape(1)
    arrived = exchange(spectra)
    gates = gate(normed, gate_weight)
    returned = exchange(length_transform(arrived, lone))
    return leave(returned, gates, out_weight)


def solution(mesh):
    return jax.shard_map(
        local,
        mesh=mesh,
        in_specs=(P(None, AXES, None), P(), P(), P(), P()),
        out_specs=P(None, AXES, None),
        check_vma=False,
    )
```

time: 125 us -> 82.6 us (0.66)
  blocking collectives: 28.4 us -> 0 us
  Pallas kernels: 0 us -> 27.8 us
  matrix products: 23.3 us -> 0 us
  local copies, waits for them, and re-layouts: 15.2 us -> 1.6 us
  other arithmetic: 4.97 us -> 0 us
  waiting for transfers between devices: 26.9 us -> 30.9 us
  starting transfers between devices: 25.7 us -> 21.8 us
    all_to_all x2 -> x0, blocking collectives: 28.4 us -> none  [exchange_in_order(): whole = lax.all_to_all(whole, axes[k], k, k, tiled=True)]
    pallas_call x0 -> x4, Pallas kernels: none -> 27.8 us  [the longest x1 8.94 us: gate(): pl.pallas_call(gate_body, grid=(steps,), in_specs=[pl.BlockSpec((SEQS * B...]
    dot_general x11 -> x0, matrix products: 23.3 us -> none  [the longest x1 6.2 us: local(): jnp.dot(normed, gate_weight, preferred_element_type=jnp.float32)]
    reshape x4 -> x0, local copies, waits for them, and re-layouts: 6.29 us -> none  [the longest x1 2.67 us: length_transform(): real_part.reshape(item_count, span_total, column_count)]
    all_to_all x3 -> x2, waiting for transfers between devices: 26.9 us -> 30.9 us  [exchange(): lax.all_to_all(x.reshape(DEVICES, ROWS, BLOCK), AXES, 0, 0, tiled=True)]
    all_to_all x3 -> x2, starting transfers between devices: 25.7 us -> 21.8 us  [exchange(): lax.all_to_all(x.reshape(DEVICES, ROWS, BLOCK), AXES, 0, 0, tiled=True)]
    convert_element_type x3 -> x0, local copies, waits for them, and re-layouts: 1.78 us -> none  [the longest x1 1.11 us: local(): jnp.dot(normed, mix_weight, preferred_element_type=jnp.float32)]
    another operation x3 -> x0, local copies, waits for them, and re-layouts: 1.71 us -> none  [the longest x1 1.33 us: local(): jnp.stack([left_part.reshape(item_count, row_count, -1), right_part.resha...]
  transfers between devices with their start and end apart: 3 -> 2, of which waited for: 3 -> 2; matrix products, arithmetic and copies ran while one was open for 6% -> 0% of each run, Pallas kernels for 0% -> 11%
where the time goes in v1:
time: 82.6 us; the launch traced here: 82.2 us
  waiting for transfers between devices  30.9 us (37%)
  Pallas kernels  27.8 us (34%)
  starting transfers between devices  21.8 us (26%)
  local copies, waits for them, and re-layouts  1.6 us (2%)
    all_to_all x2, waiting for transfers between devices, exchange(): lax.all_to_all(x.reshape(DEVICES, ROWS, BLOCK), AXES, 0, 0, tiled=True)  30.9 us
    all_to_all x2, starting transfers between devices, exchange(): lax.all_to_all(x.reshape(DEVICES, ROWS, BLOCK), AXES, 0, 0, tiled=True)  21.8 us
    pallas_call x1, Pallas kernels, gate(): pl.pallas_call(gate_body, grid=(steps,), in_specs=[pl.BlockSpec((SEQS * B...  8.94 us
    pallas_call x1, Pallas kernels, leave(): pl.pallas_call(leave_body, grid=(steps,), in_specs=[pl.BlockSpec((SEQS *...  7.89 us
    pallas_call x1, Pallas kernels, enter(): pl.pallas_call(enter_body, grid=(steps,), in_specs=[pl.BlockSpec((SEQS, B...  7.82 us
    pallas_call x1, Pallas kernels, length_transform(): pl.pallas_call(length_body, in_specs=[pl.BlockSpec(memory_space=pltpu.SME...  3.19 us
  transfers between devices with their start and end apart: 2, of which 2 were waited for; matrix products, arithmetic and copies ran while one was open for 0% of the time, Pallas kernels for 11%

profile of v1, /device:TPU:1, one launch (start us, length us, event | category | flops | bytes accessed | tf_op | source)
XLA Modules:
  0.0 82.2 jit_solution(13822091258734797207)
XLA Ops:
  0.0 7.8 %enter.1 = (bf16[2,1024,128]{2,1,0:T(8,128)(2,1)}, bf16[256,2048]{1,0:T(8,128)(2,1)}) custom-call(bf16[2,128,2048]{2,1,0:T(8,128)(2,1)} %tokens.1, f32[1,2048]{1,0:T(1,128)} %bitcast.10, bf16[2048,1024]{1,0:T(8,128)(2,1)} %weight.3, bf16[128,128]{1,0:T(8,128)(2,1)} %constant.37.clone.table), custom_call_target="tpu_custom_call" | custom-call | tf_op jit(solution)/shard_map/enter/pallas_call | solution.py:90
  7.8 15.6 %all-to-all-start = ((bf16[256,8,128]{2,1,0:T(8,128)(2,1)}), bf16[256,8,128]{2,1,0:T(8,128)(2,1)S(1)}, u32[]{:S(2)}, u32[]{:S(2)}) async-start(bf16[256,8,128]{2,1,0:T(8,128)(2,1)} %bitcast.9), calls=%async_computation | async-start | bytes 1048576 | tf_op jit(solution)/shard_map/all_to_all | solution.py:232
  23.5 19.9 %all-to-all-done = bf16[256,8,128]{2,1,0:T(8,128)(2,1)S(1)} async-done(((bf16[256,8,128]{2,1,0:T(8,128)(2,1)}), bf16[256,8,128]{2,1,0:T(8,128)(2,1)S(1)}, u32[]{:S(2)}, u32[]{:S(2)}) %all-to-all-start) | async-done | bytes 524320 | tf_op jit(solution)/shard_map/all_to_all | solution.py:232
  43.4 0.0 copy-start
  43.4 0.8 copy-done
  44.2 3.2 %length.1 = bf16[2048,128]{1,0:T(8,128)(2,1)} custom-call(f32[1]{0:T(128)} %bitcast.lone, bf16[2048,128]{1,0:T(8,128)(2,1)} %bitcast.6, bf16[512,256]{1,0:T(8,128)(2,1)} %constant.38.clone.first, f32[2,256,128]{2,1,0:T(8,128)} %constant.39.clone.twist, bf16[128,256]{1,0:T(8,128)(2,1)} %constant.40.clone.second), custom_call_target="tpu_custom_call" | custom-call | tf_op jit(solution)/shard_map/length/pallas_call | solution.py:152
  47.4 6.1 %all-to-all-start.1 = ((bf16[256,8,128]{2,1,0:T(8,128)(2,1)}), bf16[256,8,128]{2,1,0:T(8,128)(2,1)S(1)}, u32[]{:S(2)}, u32[]{:S(2)}) async-start(bf16[256,8,128]{2,1,0:T(8,128)(2,1)} %bitcast.7), calls=%async_computation.1 | async-start | bytes 1048576 | tf_op jit(solution)/shard_map/all_to_all | solution.py:232
  53.5 8.9 %gate.1.gates = f32[256,2048]{1,0:T(8,128)} custom-call(bf16[256,2048]{1,0:T(8,128)(2,1)} %get-tuple-element.8.normed, bf16[2048,2048]{1,0:T(8,128)(2,1)} %weight.4), custom_call_target="tpu_custom_call" | custom-call | flops 2147483648 | bytes 8388608 | tf_op jit(solution)/shard_map/gate/pallas_call | solution.py:176
  62.5 11.0 %all-to-all-done.1 = bf16[256,8,128]{2,1,0:T(8,128)(2,1)S(1)} async-done(((bf16[256,8,128]{2,1,0:T(8,128)(2,1)}), bf16[256,8,128]{2,1,0:T(8,128)(2,1)S(1)}, u32[]{:S(2)}, u32[]{:S(2)}) %all-to-all-start.1) | async-done | bytes 524320 | tf_op jit(solution)/shard_map/all_to_all | solution.py:232
  73.5 0.0 copy-start.1
  73.5 0.8 copy-done.1
  74.3 7.9 %leave.1 = bf16[2,128,2048]{2,1,0:T(8,128)(2,1)} custom-call(bf16[2048,128]{1,0:T(8,128)(2,1)} %bitcast.8, bf16[128,128]{1,0:T(8,128)(2,1)} %constant.41.clone.order, bf16[128,128]{1,0:T(8,128)(2,1)} %constant.42.clone.eye, bf16[1024,2048]{1,0:T(8,128)(2,1)} %weight.5, f32[256,2048]{1,0:T(8,128)} %gate.1.gates), custom_call_target="tpu_custom_call" | custom-call | tf_op jit(solution)/shard_map/leave/pallas_call | solution.py:214
Async XLA Ops:
  7.8 35.6 %all-to-all-start = ((bf16[256,8,128]{2,1,0:T(8,128)(2,1)}), bf16[256,8,128]{2,1,0:T(8,128)(2,1)S(1)}, u32[]{:S(2)}, u32[]{:S(2)}) async-start(bf16[256,8,128]{2,1,0:T(8,128)(2,1)} %bitcast.9), calls=%async_computation | async-start | bytes 1048576 | tf_op jit(solution)/shard_map/all_to_all | solution.py:232
  43.4 0.8 copy-start
  47.4 26.1 %all-to-all-start.1 = ((bf16[256,8,128]{2,1,0:T(8,128)(2,1)}), bf16[256,8,128]{2,1,0:T(8,128)(2,1)S(1)}, u32[]{:S(2)}, u32[]{:S(2)}) async-start(bf16[256,8,128]{2,1,0:T(8,128)(2,1)} %bitcast.7), calls=%async_computation.1 | async-start | bytes 1048576 | tf_op jit(solution)/shard_map/all_to_all | solution.py:232
  73.5 0.8 copy-start.1

commit v2 on v1

--- a/solution.py
+++ b/solution.py
@@ -19,6 +19,16 @@
 ROWS = 2 * PAIRS
 NT = (((1,), (1,)), ((), ()))
 F32, BF16 = jnp.float32, jnp.bfloat16
+LEAVE = 4
+SMALL = pltpu.CompilerParams(vmem_limit_bytes=16 * 2**20)
+
+
+def in_hbm(x):
+    return pltpu.with_memory_space_constraint(x, pltpu.HBM)
+
+
+def in_vmem(x):
+    return pltpu.with_memory_space_constraint(x, pltpu.VMEM)
 
 
 def group_table():
@@ -61,51 +71,63 @@
     return np.concatenate([np.cos(angle), -np.sin(angle)], axis=1) / 16
 
 
-def enter_body(tokens, gain, weight, table, out, normed):
-    @pl.when(pl.program_id(0) == 0)
-    def _():
-        for s in range(SEQS):
-
-            def rows(i, _):
-                at = pl.ds(pl.multiple_of(i * 16, 16), 16)
-                t = tokens[s, at, :].astype(F32)
-                inv = lax.rsqrt(jnp.mean(t * t, axis=-1, keepdims=True) + 1e-6)
-                to = pl.ds(pl.multiple_of(s * BLOCK + i * 16, 16), 16)
-                normed[to, :] = (t * inv * gain[...]).astype(BF16)
-                return 0
-
-            lax.fori_loop(0, BLOCK // 16, rows, 0)
-
-    mixed = jnp.dot(normed[...], weight[...], preferred_element_type=F32).astype(BF16)
-    for q in range(mixed.shape[1] // GROUP_DIM):
-        at = slice(q * GROUP_DIM, (q + 1) * GROUP_DIM)
-        turned = lax.dot_general(table[...], mixed[:, at], NT, preferred_element_type=F32)
-        for s in range(SEQS):
-            out[s, at, :] = turned[:, s * BLOCK : (s + 1) * BLOCK].astype(BF16)
+def enter_body(tokens, gain, weight, table, out, saved, held, normed, matrix, sems):
+    copies = [pltpu.make_async_copy(tokens.at[s], held.at[s], sems.at[s]) for s in range(SEQS)]
+    copies.append(pltpu.make_async_copy(weight, matrix, sems.at[SEQS]))
+    for copy in copies:
+        copy.start()
+    for s in range(SEQS):
+        copies[s].wait()
+
+        def rows(i, _):
+            at = pl.ds(pl.multiple_of(i * 16, 16), 16)
+            t = held[s, at, :].astype(F32)
+            inv = lax.rsqrt(jnp.mean(t * t, axis=-1, keepdims=True) + 1e-6)
+            to = pl.ds(pl.multiple_of(s * BLOCK + i * 16, 16), 16)
+            normed[to, :] = (t * inv * gain[...]).astype(BF16)
+            return 0
+
+        lax.fori_loop(0, BLOCK // 16, rows, 0, unroll=4)
+    save = pltpu.make_async_copy(normed, saved, sems.at[SEQS + 1])
+    save.start()
+    copies[SEQS].wait()
+    for c in range(FW // 256):
+        mixed = jnp.dot(
+            normed[...], matrix[:, c * 256 : (c + 1) * 256], preferred_element_type=F32
+        ).astype(BF16)
+        for q in range(2):
+            turned = lax.dot_general(
+                table[...],
+                mixed[:, q * GROUP_DIM : (q + 1) * GROUP_DIM],
+                NT,
+                preferred_element_type=F32,
+            )
+            at = slice(c * 256 + q * GROUP_DIM, c * 256 + (q + 1) * GROUP_DIM)
+            for s in range(SEQS):
+                out[s, at, :] = turned[:, s * BLOCK : (s + 1) * BLOCK].astype(BF16)
+    save.wait()
 
 
 def enter(tokens, gain, weight):
-    steps = 4
-    wide = FW // steps
+    vmem = pl.BlockSpec(memory_space=pltpu.VMEM)
+    hbm = pl.BlockSpec(memory_space=pltpu.HBM)
     return pl.pallas_call(
         enter_body,
-        grid=(steps,),
-        in_specs=[
-            pl.BlockSpec((SEQS, BLOCK, D), lambda j: (0, 0, 0)),
-            pl.BlockSpec((1, D), lambda j: (0, 0)),
-            pl.BlockSpec((D, wide), lambda j: (0, j)),
-            pl.BlockSpec((GROUP_DIM, GROUP_DIM), lambda j: (0, 0)),
-        ],
-        out_specs=[
-            pl.BlockSpec((SEQS, wide, BLOCK), lambda j: (0, j, 0)),
-            pl.BlockSpec((SEQS * BLOCK, D), lambda j: (0, 0)),
-        ],
+        in_specs=[hbm, vmem, hbm, vmem],
+        out_specs=[vmem, hbm],
         out_shape=[
             jax.ShapeDtypeStruct((SEQS, FW, BLOCK), BF16),
-            jax.ShapeDtypeStruct((SEQS * BLOCK, D), BF16),
-        ],
+            pltpu.HBM((SEQS * BLOCK, D), BF16),
+        ],
+        scratch_shapes=[
+            pltpu.VMEM((SEQS, BLOCK, D), BF16),
+            pltpu.VMEM((SEQS * BLOCK, D), BF16),
+            pltpu.VMEM((D, FW), BF16),
+            pltpu.SemaphoreType.DMA((SEQS + 2,)),
+        ],
+        compiler_params=SMALL,
         name="enter",
-    )(tokens, gain.reshape(1, D), weight, jnp.asarray(group_table(), BF16))
+    )(in_hbm(tokens), gain.reshape(1, D), in_hbm(weight), jnp.asarray(group_table(), BF16))
 
 
 def length_body(lone, x, first, twist, second, y, wide_in, wide_out):
@@ -155,6 +177,7 @@
         out_specs=vmem,
         out_shape=jax.ShapeDtypeStruct((rows, BLOCK), BF16),
         scratch_shapes=[pltpu.VMEM((rows, BLOCK), F32), pltpu.VMEM((rows, BLOCK), F32)],
+        compiler_params=SMALL,
         name="length",
     )(
         lone,
@@ -181,51 +204,64 @@
             pl.BlockSpec((D, wide), lambda j: (0, j)),
         ],
         out_specs=pl.BlockSpec((SEQS * BLOCK, wide), lambda j: (0, j)),
-        out_shape=jax.ShapeDtypeStruct((SEQS * BLOCK, D), F32),
+        out_shape=pltpu.VMEM((SEQS * BLOCK, D), F32),
         cost_estimate=pl.CostEstimate(
             flops=2 * SEQS * BLOCK * D * D, transcendentals=SEQS * BLOCK * D, bytes_accessed=2 * D * D
         ),
+        compiler_params=SMALL,
         name="gate",
-    )(normed, weight)
-
-
-def leave_body(z, order, eye, weight, gates, out, spectral):
-    @pl.when(pl.program_id(0) == 0)
-    def _():
+    )(in_hbm(normed), in_hbm(weight))
+
+
+def leave_body(z, order, eye, weight, gates, out, matrix, spectral, gated, sems, arrive):
+    wide = D // LEAVE
+    loads = []
+    for c in range(LEAVE):
+        at = slice(c * wide, (c + 1) * wide)
+        load = pltpu.make_async_copy(weight.at[:, at], matrix.at[:, at], arrive.at[c])
+        load.start()
+        loads.append(load)
+    for s in range(SEQS):
+        for g in range(GROUPS):
+            rows = z[s * FW + g * GROUP_DIM : s * FW + (g + 1) * GROUP_DIM, :]
+            turned = lax.dot_general(eye[...], rows, NT, preferred_element_type=F32)
+            placed = jnp.dot(turned.astype(BF16), order[...], preferred_element_type=F32)
+            spectral[s * BLOCK : (s + 1) * BLOCK, g * GROUP_DIM : (g + 1) * GROUP_DIM] = (
+                placed.astype(BF16)
+            )
+    copies = []
+    for c in range(LEAVE):
+        at = slice(c * wide, (c + 1) * wide)
+        loads[c].wait()
+        mapped = jnp.dot(spectral[...], matrix[:, at], preferred_element_type=F32)
+        block = (gates[:, at] * mapped).astype(BF16)
         for s in range(SEQS):
-            for g in range(GROUPS):
-                rows = z[pl.ds(s * FW + g * GROUP_DIM, GROUP_DIM), :]
-                turned = lax.dot_general(eye[...], rows, NT, preferred_element_type=F32)
-                placed = jnp.dot(turned.astype(BF16), order[...], preferred_element_type=F32)
-                spectral[s * BLOCK : (s + 1) * BLOCK, g * GROUP_DIM : (g + 1) * GROUP_DIM] = (
-                    placed.astype(BF16)
-                )
-
-    mapped = jnp.dot(spectral[...], weight[...], preferred_element_type=F32)
-    gated = (gates[...] * mapped).astype(BF16)
-    for s in range(SEQS):
-        out[s] = gated[s * BLOCK : (s + 1) * BLOCK]
+            gated[s, :, at] = block[s * BLOCK : (s + 1) * BLOCK]
+        copy = pltpu.make_async_copy(gated.at[:, :, at], out.at[:, :, at], sems.at[c])
+        copy.start()
+        copies.append(copy)
+    for copy in copies:
+        copy.wait()
 
 
 def leave(z, gates, weight):
-    steps = 4
-    wide = D // steps
-    square = pl.BlockSpec((GROUP_DIM, GROUP_DIM), lambda j: (0, 0))
+    vmem = pl.BlockSpec(memory_space=pltpu.VMEM)
+    hbm = pl.BlockSpec(memory_space=pltpu.HBM)
     return pl.pallas_call(
         leave_body,
-        grid=(steps,),
-        in_specs=[
-            pl.BlockSpec((SEQS * FW, BLOCK), lambda j: (0, 0)),
-            square,
-            square,
-            pl.BlockSpec((FW, wide), lambda j: (0, j)),
-            pl.BlockSpec((SEQS * BLOCK, wide), lambda j: (0, j)),
-        ],
-        out_specs=pl.BlockSpec((SEQS, BLOCK, wide), lambda j: (0, 0, j)),
+        in_specs=[vmem, vmem, vmem, hbm, vmem],
+        out_specs=hbm,
         out_shape=jax.ShapeDtypeStruct((SEQS, BLOCK, D), BF16),
-        scratch_shapes=[pltpu.VMEM((SEQS * BLOCK, FW), BF16)],
+        scratch_shapes=[
+            pltpu.VMEM((FW, D), BF16),
+            pltpu.VMEM((SEQS * BLOCK, FW), BF16),
+            pltpu.VMEM((SEQS, BLOCK, D), BF16),
+            pltpu.SemaphoreType.DMA((LEAVE,)),
+            pltpu.SemaphoreType.DMA((LEAVE,)),
+        ],
+        compiler_params=SMALL,
         name="leave",
-    )(z, jnp.asarray(channel_order(), BF16), jnp.asarray(np.eye(GROUP_DIM), BF16), weight, gates)
+    )(z, jnp.asarray(channel_order(), BF16), jnp.asarray(np.eye(GROUP_DIM), BF16), in_hbm(weight), in_vmem(gates))
 
 
 def exchange(x):
@@ -237,6 +273,7 @@
 def local(tokens, norm_gain, mix_weight, gate_weight, out_weight):
     spectra, normed = enter(tokens, norm_gain, mix_weight)
     lone = (lax.axis_index(AXES) % (GROUP_DIM // ROWS) == 0).astype(F32).reshape(1)
+    spectra, lone = lax.optimization_barrier((spectra, lone))
     arrived = exchange(spectra)
     gates = gate(normed, gate_weight)
     returned = exchange(length_transform(arrived, lone))

time: 82.6 us -> 77 us (0.932)
  blocking collectives: 0 us -> 35.4 us
  waiting for transfers between devices: 30.9 us -> 12.1 us
  starting transfers between devices: 21.8 us -> 6.12 us
  Pallas kernels: 27.8 us -> 21.4 us
    all_to_all x0 -> x1, blocking collectives: none -> 35.4 us  [exchange(): lax.all_to_all(x.reshape(DEVICES, ROWS, BLOCK), AXES, 0, 0, tiled=True)]
    all_to_all x2 -> x1, waiting for transfers between devices: 30.9 us -> 12.1 us  [exchange(): lax.all_to_all(x.reshape(DEVICES, ROWS, BLOCK), AXES, 0, 0, tiled=True)]
    all_to_all x2 -> x1, starting transfers between devices: 21.8 us -> 6.12 us  [exchange(): lax.all_to_all(x.reshape(DEVICES, ROWS, BLOCK), AXES, 0, 0, tiled=True)]
    pallas_call x2, Pallas kernels: 15.7 us -> 11.6 us  [the longest x1 6.04 us: leave(): pl.pallas_call(leave_body, in_specs=[vmem, vmem, vmem, hbm, vmem], out_sp...]
    pallas_call x1, Pallas kernels: 3.19 us -> 2 us  [length_transform(): pl.pallas_call(length_body, in_specs=[pl.BlockSpec(memory_space=pltpu.SME...]
    pallas_call x1, Pallas kernels: 8.94 us -> 7.8 us  [gate(): pl.pallas_call(gate_body, grid=(steps,), in_specs=[pl.BlockSpec((SEQS * B...]
  transfers between devices with their start and end apart: 2 -> 1, of which waited for: 2 -> 1; matrix products, arithmetic and copies ran while one was open for 0% -> 0% of each run, Pallas kernels for 11% -> 10%
where the time goes in v2:
time: 77 us; the launch traced here: 76.7 us
  blocking collectives  35.4 us (46%)
  Pallas kernels  21.4 us (28%)
  waiting for transfers between devices  12.1 us (16%)
  starting transfers between devices  6.12 us (8%)
  local copies, waits for them, and re-layouts  1.53 us (2%)
    all_to_all x1, blocking collectives, exchange(): lax.all_to_all(x.reshape(DEVICES, ROWS, BLOCK), AXES, 0, 0, tiled=True)  35.4 us
    all_to_all x1, waiting for transfers between devices, exchange(): lax.all_to_all(x.reshape(DEVICES, ROWS, BLOCK), AXES, 0, 0, tiled=True)  12.1 us
    pallas_call x1, Pallas kernels, gate(): pl.pallas_call(gate_body, grid=(steps,), in_specs=[pl.BlockSpec((SEQS * B...  7.8 us
    all_to_all x1, starting transfers between devices, exchange(): lax.all_to_all(x.reshape(DEVICES, ROWS, BLOCK), AXES, 0, 0, tiled=True)  6.12 us
    pallas_call x1, Pallas kernels, leave(): pl.pallas_call(leave_body, in_specs=[vmem, vmem, vmem, hbm, vmem], out_sp...  6.04 us
    pallas_call x1, Pallas kernels, enter(): pl.pallas_call(enter_body, in_specs=[hbm, vmem, hbm, vmem], out_specs=[vm...  5.61 us
    pallas_call x1, Pallas kernels, length_transform(): pl.pallas_call(length_body, in_specs=[pl.BlockSpec(memory_space=pltpu.SME...  2 us
  transfers between devices with their start and end apart: 1, of which 1 were waited for; matrix products, arithmetic and copies ran while one was open for 0% of the time, Pallas kernels for 10%

profile of v2, /device:TPU:1, one launch (start us, length us, event | category | flops | bytes accessed | tf_op | source)
XLA Modules:
  0.0 76.7 jit_solution(14056454151114898265)
XLA Ops:
  0.0 0.0 copy-start.2
  0.0 0.0 copy-start
  0.0 0.0 copy-start.1
  0.0 0.0 copy-start.5
  0.0 0.8 %copy-done.5 = bf16[128,128]{1,0:T(8,128)(2,1)S(1)} copy-done((bf16[128,128]{1,0:T(8,128)(2,1)S(1)}, bf16[128,128]{1,0:T(8,128)(2,1)}, u32[]{:S(2)}) %copy-start.5) | copy-done | bytes 32792
  0.8 0.0 copy-start.6
  0.8 0.7 copy-done.6
  1.5 5.6 %enter.1 = (bf16[2,1024,128]{2,1,0:T(8,128)(2,1)S(1)}, bf16[256,2048]{1,0:T(8,128)(2,1)}) custom-call(bf16[2,128,2048]{2,1,0:T(8,128)(2,1)} %tokens.1, f32[1,2048]{1,0:T(1,128)S(1)} %bitcast.9, bf16[2048,1024]{1,0:T(8,128)(2,1)} %weight.3, bf16[128,128]{1,0:T(8,128)(2,1)S(1)} %copy-done.5), custom_call_target="tpu_custom_call" | custom-call | tf_op jit(solution)/shard_map/enter/pallas_call | solution.py:114
  7.2 35.4 %all_to_all.10 = bf16[256,8,128]{2,1,0:T(8,128)(2,1)S(1)} all-to-all(bf16[256,8,128]{2,1,0:T(8,128)(2,1)S(1)} %bitcast.8), channel_id=1, replica_groups=mesh['row'=32,'col'=8] {'row','col'}, dimensions={0} | all-to-all | bytes 1048576 | tf_op jit(solution)/shard_map/all_to_all | solution.py:268
  42.6 0.0 copy-done.2
  42.6 0.0 copy-done
  42.6 0.0 copy-done.1
  42.6 2.0 %length.1 = bf16[2048,128]{1,0:T(8,128)(2,1)} custom-call(f32[1]{0:T(128)} %bitcast.1.lone, bf16[2048,128]{1,0:T(8,128)(2,1)S(1)} %bitcast.6, bf16[512,256]{1,0:T(8,128)(2,1)S(1)} %copy-done.1, f32[2,256,128]{2,1,0:T(8,128)S(1)} %copy-done, bf16[128,256]{1,0:T(8,128)(2,1)S(1)} %copy-done.2), custom_call_target="tpu_custom_call" | custom-call | tf_op jit(solution)/shard_map/length/pallas_call | solution.py:174
  44.6 6.1 %all-to-all-start.1 = ((bf16[256,8,128]{2,1,0:T(8,128)(2,1)}), bf16[256,8,128]{2,1,0:T(8,128)(2,1)S(1)}, u32[]{:S(2)}, u32[]{:S(2)}) async-start(bf16[256,8,128]{2,1,0:T(8,128)(2,1)} %bitcast.4), calls=%async_computation.1 | async-start | bytes 1048576 | tf_op jit(solution)/shard_map/all_to_all | solution.py:268
  50.7 0.0 copy-start.3
  50.7 0.0 copy-start.4
  50.7 7.8 %gate.1.gates = f32[256,2048]{1,0:T(8,128)S(1)} custom-call(bf16[256,2048]{1,0:T(8,128)(2,1)} %get-tuple-element.12.normed, bf16[2048,2048]{1,0:T(8,128)(2,1)} %weight.4), custom_call_target="tpu_custom_call" | custom-call | flops 2147483648 | bytes 8388608 | tf_op jit(solution)/shard_map/gate/pallas_call | solution.py:199
  58.5 12.1 %all-to-all-done.1 = bf16[256,8,128]{2,1,0:T(8,128)(2,1)S(1)} async-done(((bf16[256,8,128]{2,1,0:T(8,128)(2,1)}), bf16[256,8,128]{2,1,0:T(8,128)(2,1)S(1)}, u32[]{:S(2)}, u32[]{:S(2)}) %all-to-all-start.1) | async-done | bytes 524320 | tf_op jit(solution)/shard_map/all_to_all | solution.py:268
  70.6 0.0 copy-done.3
  70.6 0.0 copy-done.4
  70.6 6.0 %leave.1 = bf16[2,128,2048]{2,1,0:T(8,128)(2,1)} custom-call(bf16[2048,128]{1,0:T(8,128)(2,1)S(1)} %bitcast.7, bf16[128,128]{1,0:T(8,128)(2,1)S(1)} %copy-done.4, bf16[128,128]{1,0:T(8,128)(2,1)S(1)} %copy-done.3, bf16[1024,2048]{1,0:T(8,128)(2,1)} %weight.5, f32[256,2048]{1,0:T(8,128)S(1)} %gate.1.gates), custom_call_target="tpu_custom_call" | custom-call | tf_op jit(solution)/shard_map/leave/pallas_call | solution.py:250
Async XLA Ops:
  0.0 42.6 %copy-start.2 = (bf16[128,256]{1,0:T(8,128)(2,1)S(1)}, bf16[128,256]{1,0:T(8,128)(2,1)}, u32[]{:S(2)}) copy-start(bf16[128,256]{1,0:T(8,128)(2,1)} %constant.40.clone.second) | copy-start | bytes 196612
  0.0 42.6 %copy-start = (f32[2,256,128]{2,1,0:T(8,128)S(1)}, f32[2,256,128]{2,1,0:T(8,128)}, u32[]{:S(2)}) copy-start(f32[2,256,128]{2,1,0:T(8,128)} %constant.39.clone.twist) | copy-start | bytes 786436
  0.0 42.6 %copy-start.1 = (bf16[512,256]{1,0:T(8,128)(2,1)S(1)}, bf16[512,256]{1,0:T(8,128)(2,1)}, u32[]{:S(2)}) copy-start(bf16[512,256]{1,0:T(8,128)(2,1)} %constant.38.clone.first) | copy-start | bytes 786436
  0.0 0.8 %copy-start.5 = (bf16[128,128]{1,0:T(8,128)(2,1)S(1)}, bf16[128,128]{1,0:T(8,128)(2,1)}, u32[]{:S(2)}) copy-start(bf16[128,128]{1,0:T(8,128)(2,1)} %constant.37.clone.table) | copy-start | bytes 98308
  0.8 0.7 copy-start.6
  44.6 26.1 %all-to-all-start.1 = ((bf16[256,8,128]{2,1,0:T(8,128)(2,1)}), bf16[256,8,128]{2,1,0:T(8,128)(2,1)S(1)}, u32[]{:S(2)}, u32[]{:S(2)}) async-start(bf16[256,8,128]{2,1,0:T(8,128)(2,1)} %bitcast.4), calls=%async_computation.1 | async-start | bytes 1048576 | tf_op jit(solution)/shard_map/all_to_all | solution.py:268
  50.7 19.9 %copy-start.3 = (bf16[128,128]{1,0:T(8,128)(2,1)S(1)}, bf16[128,128]{1,0:T(8,128)(2,1)}, u32[]{:S(2)}) copy-start(bf16[128,128]{1,0:T(8,128)(2,1)} %constant.42.clone.eye) | copy-start | bytes 98308
  50.7 19.9 %copy-start.4 = (bf16[128,128]{1,0:T(8,128)(2,1)S(1)}, bf16[128,128]{1,0:T(8,128)(2,1)}, u32[]{:S(2)}) copy-start(bf16[128,128]{1,0:T(8,128)(2,1)} %constant.41.clone.order) | copy-start | bytes 98308

commit v3 on v2

--- a/solution.py
+++ b/solution.py
@@ -20,6 +20,7 @@
 NT = (((1,), (1,)), ((), ()))
 F32, BF16 = jnp.float32, jnp.bfloat16
 LEAVE = 4
+ENTER = 256
 SMALL = pltpu.CompilerParams(vmem_limit_bytes=16 * 2**20)
 
 
@@ -71,38 +72,42 @@
     return np.concatenate([np.cos(angle), -np.sin(angle)], axis=1) / 16
 
 
-def enter_body(tokens, gain, weight, table, out, saved, held, normed, matrix, sems):
-    copies = [pltpu.make_async_copy(tokens.at[s], held.at[s], sems.at[s]) for s in range(SEQS)]
-    copies.append(pltpu.make_async_copy(weight, matrix, sems.at[SEQS]))
-    for copy in copies:
+def enter_body(tokens, gain, weight, table, out, saved, held, scale, turn, normed, matrix, sems):
+    def load(source, target, at):
+        copy = pltpu.make_async_copy(source, target, sems.at[at])
         copy.start()
+        return copy
+
+    small = [load(gain, scale, 0), load(table, turn, 1)]
+    rows_in = [load(tokens.at[s], held.at[s], 2 + s) for s in range(SEQS)]
+    cuts = [slice(c * ENTER, (c + 1) * ENTER) for c in range(FW // ENTER)]
+    chunks = [load(weight.at[:, cut], matrix.at[:, cut], 4 + c) for c, cut in enumerate(cuts)]
+    for copy in small:
+        copy.wait()
     for s in range(SEQS):
-        copies[s].wait()
+        rows_in[s].wait()
 
         def rows(i, _):
             at = pl.ds(pl.multiple_of(i * 16, 16), 16)
             t = held[s, at, :].astype(F32)
             inv = lax.rsqrt(jnp.mean(t * t, axis=-1, keepdims=True) + 1e-6)
             to = pl.ds(pl.multiple_of(s * BLOCK + i * 16, 16), 16)
-            normed[to, :] = (t * inv * gain[...]).astype(BF16)
+            normed[to, :] = (t * inv * scale[...]).astype(BF16)
             return 0
 
         lax.fori_loop(0, BLOCK // 16, rows, 0, unroll=4)
-    save = pltpu.make_async_copy(normed, saved, sems.at[SEQS + 1])
-    save.start()
-    copies[SEQS].wait()
-    for c in range(FW // 256):
-        mixed = jnp.dot(
-            normed[...], matrix[:, c * 256 : (c + 1) * 256], preferred_element_type=F32
-        ).astype(BF16)
-        for q in range(2):
+    save = load(normed, saved, 4 + len(cuts))
+    for chunk, cut in zip(chunks, cuts):
+        chunk.wait()
+        mixed = jnp.dot(normed[...], matrix[:, cut], preferred_element_type=F32).astype(BF16)
+        for q in range(ENTER // GROUP_DIM):
             turned = lax.dot_general(
-                table[...],
+                turn[...],
                 mixed[:, q * GROUP_DIM : (q + 1) * GROUP_DIM],
                 NT,
                 preferred_element_type=F32,
             )
-            at = slice(c * 256 + q * GROUP_DIM, c * 256 + (q + 1) * GROUP_DIM)
+            at = slice(cut.start + q * GROUP_DIM, cut.start + (q + 1) * GROUP_DIM)
             for s in range(SEQS):
                 out[s, at, :] = turned[:, s * BLOCK : (s + 1) * BLOCK].astype(BF16)
     save.wait()
@@ -113,7 +118,7 @@
     hbm = pl.BlockSpec(memory_space=pltpu.HBM)
     return pl.pallas_call(
         enter_body,
-        in_specs=[hbm, vmem, hbm, vmem],
+        in_specs=[hbm] * 4,
         out_specs=[vmem, hbm],
         out_shape=[
             jax.ShapeDtypeStruct((SEQS, FW, BLOCK), BF16),
@@ -121,18 +126,35 @@
         ],
         scratch_shapes=[
             pltpu.VMEM((SEQS, BLOCK, D), BF16),
+            pltpu.VMEM((1, D), F32),
+            pltpu.VMEM((GROUP_DIM, GROUP_DIM), BF16),
             pltpu.VMEM((SEQS * BLOCK, D), BF16),
             pltpu.VMEM((D, FW), BF16),
-            pltpu.SemaphoreType.DMA((SEQS + 2,)),
+            pltpu.SemaphoreType.DMA((5 + FW // ENTER,)),
         ],
         compiler_params=SMALL,
         name="enter",
-    )(in_hbm(tokens), gain.reshape(1, D), in_hbm(weight), jnp.asarray(group_table(), BF16))
-
-
-def length_body(lone, x, first, twist, second, y, wide_in, wide_out):
+    )(
+        in_hbm(tokens),
+        in_hbm(gain.reshape(1, D)),
+        in_hbm(weight),
+        in_hbm(jnp.asarray(group_table(), BF16)),
+    )
+
+
+def length_body(lone, x, first, twist, second, later, y, kept, wide_in, wide_out, sem):
+    load = pltpu.make_async_copy(later, kept, sem)
+    load.start()
+
+    @pl.when(lone[0] >= 0)
+    def _():
+        over_positions(lone[0], x, first, twist, second, y, wide_in, wide_out)
+
+    load.wait()
+
+
+def over_positions(own, x, first, twist, second, y, wide_in, wide_out):
     wide_in[...] = x[...].astype(F32)
-    own = lone[0]
     cos, sin = twist[0], twist[1]
     for p in range(PAIRS):
         pair = jnp.concatenate(
@@ -168,15 +190,26 @@
     y[...] = wide_out[...].astype(BF16)
 
 
-def length_transform(x, lone):
+def length_transform(x, lone, later):
     vmem = pl.BlockSpec(memory_space=pltpu.VMEM)
     rows = DEVICES * ROWS
     return pl.pallas_call(
         length_body,
-        in_specs=[pl.BlockSpec(memory_space=pltpu.SMEM), vmem, vmem, vmem, vmem],
-        out_specs=vmem,
-        out_shape=jax.ShapeDtypeStruct((rows, BLOCK), BF16),
-        scratch_shapes=[pltpu.VMEM((rows, BLOCK), F32), pltpu.VMEM((rows, BLOCK), F32)],
+        in_specs=[
+            pl.BlockSpec(memory_space=pltpu.SMEM),
+            vmem,
+            vmem,
+            vmem,
+            vmem,
+            pl.BlockSpec(memory_space=pltpu.HBM),
+        ],
+        out_specs=[vmem, vmem],
+        out_shape=[jax.ShapeDtypeStruct((rows, BLOCK), BF16), pltpu.VMEM(later.shape, BF16)],
+        scratch_shapes=[
+            pltpu.VMEM((rows, BLOCK), F32),
+            pltpu.VMEM((rows, BLOCK), F32),
+            pltpu.SemaphoreType.DMA,
+        ],
         compiler_params=SMALL,
         name="length",
     )(
@@ -185,6 +218,7 @@
         jnp.asarray(first_table(), BF16),
         jnp.asarray(twiddle(), F32),
         jnp.asarray(second_table(), BF16),
+        in_hbm(later),
     )
 
 
@@ -213,27 +247,25 @@
     )(in_hbm(normed), in_hbm(weight))
 
 
-def leave_body(z, order, eye, weight, gates, out, matrix, spectral, gated, sems, arrive):
+def leave_body(z, order, eye, weight, gates, out, spectral, gated, sems):
+    two = 2 * GROUP_DIM
+    for g in range(FW // two):
+        turned = [
+            lax.dot_general(
+                eye[...],
+                z[s * FW + g * two : s * FW + (g + 1) * two, :],
+                NT,
+                preferred_element_type=F32,
+            ).astype(BF16)
+            for s in range(SEQS)
+        ]
+        placed = jnp.dot(jnp.concatenate(turned, axis=0), order[...], preferred_element_type=F32)
+        spectral[:, g * two : (g + 1) * two] = placed.astype(BF16)
+    copies = []
     wide = D // LEAVE
-    loads = []
     for c in range(LEAVE):
         at = slice(c * wide, (c + 1) * wide)
-        load = pltpu.make_async_copy(weight.at[:, at], matrix.at[:, at], arrive.at[c])
-        load.start()
-        loads.append(load)
-    for s in range(SEQS):
-        for g in range(GROUPS):
-            rows = z[s * FW + g * GROUP_DIM : s * FW + (g + 1) * GROUP_DIM, :]
-            turned = lax.dot_general(eye[...], rows, NT, preferred_element_type=F32)
-            placed = jnp.dot(turned.astype(BF16), order[...], preferred_element_type=F32)
-            spectral[s * BLOCK : (s + 1) * BLOCK, g * GROUP_DIM : (g + 1) * GROUP_DIM] = (
-                placed.astype(BF16)
-            )
-    copies = []
-    for c in range(LEAVE):
-        at = slice(c * wide, (c + 1) * wide)
-        loads[c].wait()
-        mapped = jnp.dot(spectral[...], matrix[:, at], preferred_element_type=F32)
+        mapped = jnp.dot(spectral[...], weight[:, at], preferred_element_type=F32)
         block = (gates[:, at] * mapped).astype(BF16)
         for s in range(SEQS):
             gated[s, :, at] = block[s * BLOCK : (s + 1) * BLOCK]
@@ -246,22 +278,25 @@
 
 def leave(z, gates, weight):
     vmem = pl.BlockSpec(memory_space=pltpu.VMEM)
-    hbm = pl.BlockSpec(memory_space=pltpu.HBM)
     return pl.pallas_call(
         leave_body,
-        in_specs=[vmem, vmem, vmem, hbm, vmem],
-        out_specs=hbm,
+        in_specs=[vmem] * 5,
+        out_specs=pl.BlockSpec(memory_space=pltpu.HBM),
         out_shape=jax.ShapeDtypeStruct((SEQS, BLOCK, D), BF16),
         scratch_shapes=[
-            pltpu.VMEM((FW, D), BF16),
             pltpu.VMEM((SEQS * BLOCK, FW), BF16),
             pltpu.VMEM((SEQS, BLOCK, D), BF16),
             pltpu.SemaphoreType.DMA((LEAVE,)),
-            pltpu.SemaphoreType.DMA((LEAVE,)),
         ],
         compiler_params=SMALL,
         name="leave",
-    )(z, jnp.asarray(channel_order(), BF16), jnp.asarray(np.eye(GROUP_DIM), BF16), in_hbm(weight), in_vmem(gates))
+    )(
+        z,
+        jnp.asarray(np.kron(np.eye(2), channel_order()), BF16),
+        jnp.asarray(np.eye(GROUP_DIM), BF16),
+        in_vmem(weight),
+        in_vmem(gates),
+    )
 
 
 def exchange(x):
@@ -273,11 +308,10 @@
 def local(tokens, norm_gain, mix_weight, gate_weight, out_weight):
     spectra, normed = enter(tokens, norm_gain, mix_weight)
     lone = (lax.axis_index(AXES) % (GROUP_DIM // ROWS) == 0).astype(F32).reshape(1)
-    spectra, lone = lax.optimization_barrier((spectra, lone))
     arrived = exchange(spectra)
-    gates = gate(normed, gate_weight)
-    returned = exchange(length_transform(arrived, lone))
-    return leave(returned, gates, out_weight)
+    arrived, gates = lax.optimization_barrier((arrived, gate(normed, gate_weight)))
+    turned, matrix = length_transform(arrived, lone, out_weight)
+    return leave(exchange(turned), gates, matrix)
 
 
 def solution(mesh):

time: 77 us -> 72.5 us (0.942)
  starting transfers between devices: 6.12 us -> 15.7 us
  blocking collectives: 35.4 us -> 25.9 us
  Pallas kernels: 21.4 us -> 18.6 us
  local copies, waits for them, and re-layouts: 1.53 us -> 0.03 us
    all_to_all x1, starting transfers between devices: 6.12 us -> 15.7 us  [exchange(): lax.all_to_all(x.reshape(DEVICES, ROWS, BLOCK), AXES, 0, 0, tiled=True)]
    all_to_all x1, blocking collectives: 35.4 us -> 25.9 us  [exchange(): lax.all_to_all(x.reshape(DEVICES, ROWS, BLOCK), AXES, 0, 0, tiled=True)]
    pallas_call x2, Pallas kernels: 11.6 us -> 8.51 us  [the longest x1 6.1 us: enter(): pl.pallas_call(enter_body, in_specs=[hbm] * 4, out_specs=[vmem, hbm], out...]
    unnamed x14 -> x10, local copies, waits for them, and re-layouts: 1.53 us -> 0.03 us
  transfers between devices with their start and end apart: 1 -> 1, of which waited for: 1 -> 1; matrix products, arithmetic and copies ran while one was open for 0% -> 0% of each run, Pallas kernels for 10% -> 11%
where the time goes in v3:
time: 72.5 us; the launch traced here: 72.2 us
  blocking collectives  25.9 us (36%)
  Pallas kernels  18.6 us (26%)
  starting transfers between devices  15.7 us (22%)
  waiting for transfers between devices  12 us (17%)
    all_to_all x1, blocking collectives, exchange(): lax.all_to_all(x.reshape(DEVICES, ROWS, BLOCK), AXES, 0, 0, tiled=True)  25.9 us
    all_to_all x1, starting transfers between devices, exchange(): lax.all_to_all(x.reshape(DEVICES, ROWS, BLOCK), AXES, 0, 0, tiled=True)  15.7 us
    all_to_all x1, waiting for transfers between devices, exchange(): lax.all_to_all(x.reshape(DEVICES, ROWS, BLOCK), AXES, 0, 0, tiled=True)  12 us
    pallas_call x1, Pallas kernels, gate(): pl.pallas_call(gate_body, grid=(steps,), in_specs=[pl.BlockSpec((SEQS * B...  7.85 us
    pallas_call x1, Pallas kernels, enter(): pl.pallas_call(enter_body, in_specs=[hbm] * 4, out_specs=[vmem, hbm], out...  6.1 us
    pallas_call x1, Pallas kernels, leave(): pl.pallas_call(leave_body, in_specs=[vmem] * 5, out_specs=pl.BlockSpec(me...  2.41 us
    pallas_call x1, Pallas kernels, length_transform(): pl.pallas_call(length_body, in_specs=[pl.BlockSpec(memory_space=pltpu.SME...  2.2 us
  transfers between devices with their start and end apart: 1, of which 1 were waited for; matrix products, arithmetic and copies ran while one was open for 0% of the time, Pallas kernels for 11%

profile of v3, /device:TPU:1, one launch (start us, length us, event | category | flops | bytes accessed | tf_op | source)
XLA Modules:
  0.0 72.2 jit_solution(17875426858544370497)
XLA Ops:
  0.0 6.1 %enter.1 = (bf16[2,1024,128]{2,1,0:T(8,128)(2,1)}, bf16[256,2048]{1,0:T(8,128)(2,1)}) custom-call(bf16[2,128,2048]{2,1,0:T(8,128)(2,1)} %tokens.1, f32[1,2048]{1,0:T(1,128)} %bitcast.9, bf16[2048,1024]{1,0:T(8,128)(2,1)} %weight.2, bf16[128,128]{1,0:T(8,128)(2,1)} %constant.37.clone.table), custom_call_target="tpu_custom_call" | custom-call | tf_op jit(solution)/shard_map/enter/pallas_call | solution.py:119
  6.1 15.7 %all-to-all-start = ((bf16[256,8,128]{2,1,0:T(8,128)(2,1)}), bf16[256,8,128]{2,1,0:T(8,128)(2,1)S(1)}, u32[]{:S(2)}, u32[]{:S(2)}) async-start(bf16[256,8,128]{2,1,0:T(8,128)(2,1)} %bitcast.2), calls=%async_computation | async-start | bytes 1048576 | tf_op jit(solution)/shard_map/all_to_all | solution.py:303
  21.8 0.0 copy-start
  21.8 0.0 copy-start.1
  21.8 0.0 copy-start.3
  21.8 7.8 %gate.1.gates = f32[256,2048]{1,0:T(8,128)S(1)} custom-call(bf16[256,2048]{1,0:T(8,128)(2,1)} %get-tuple-element.12.normed, bf16[2048,2048]{1,0:T(8,128)(2,1)} %weight.3), custom_call_target="tpu_custom_call" | custom-call | flops 2147483648 | bytes 8388608 | tf_op jit(solution)/shard_map/gate/pallas_call | solution.py:233
  29.7 0.0 copy-start.2
  29.7 0.0 copy-start.4
  29.7 12.0 %all-to-all-done = bf16[256,8,128]{2,1,0:T(8,128)(2,1)S(1)} async-done(((bf16[256,8,128]{2,1,0:T(8,128)(2,1)}), bf16[256,8,128]{2,1,0:T(8,128)(2,1)S(1)}, u32[]{:S(2)}, u32[]{:S(2)}) %all-to-all-start) | async-done | bytes 524320 | tf_op jit(solution)/shard_map/all_to_all | solution.py:303
  41.7 0.0 copy-done
  41.7 0.0 copy-done.1
  41.7 0.0 copy-done.3
  41.7 2.2 %length.1 = (bf16[2048,128]{1,0:T(8,128)(2,1)S(1)}, bf16[1024,2048]{1,0:T(8,128)(2,1)S(1)}) custom-call(f32[1]{0:T(128)} %bitcast.lone, bf16[2048,128]{1,0:T(8,128)(2,1)S(1)} %bitcast.6, bf16[512,256]{1,0:T(8,128)(2,1)S(1)} %copy-done.1, f32[2,256,128]{2,1,0:T(8,128)S(1)} %copy-done, bf16[128,256]{1,0:T(8,128)(2,1)S(1)} %copy-done.3, bf16[1024,2048]{1,0:T(8,128)(2,1)} %later.1), custom_call_target="tpu_custom_call" | custom-call | tf_op jit(solution)/shard_map/length/pallas_call | solution.py:196
  43.9 25.9 %all_to_all.10 = bf16[256,8,128]{2,1,0:T(8,128)(2,1)S(1)} all-to-all(bf16[256,8,128]{2,1,0:T(8,128)(2,1)S(1)} %bitcast.8), channel_id=1, replica_groups=mesh['row'=32,'col'=8] {'row','col'}, dimensions={0} | all-to-all | bytes 1048576 | tf_op jit(solution)/shard_map/all_to_all | solution.py:303
  69.8 0.0 copy-done.2
  69.8 0.0 copy-done.4
  69.8 2.4 %leave.1 = bf16[2,128,2048]{2,1,0:T(8,128)(2,1)} custom-call(bf16[2048,128]{1,0:T(8,128)(2,1)S(1)} %bitcast.7, bf16[256,256]{1,0:T(8,128)(2,1)S(1)} %copy-done.2, bf16[128,128]{1,0:T(8,128)(2,1)S(1)} %copy-done.4, bf16[1024,2048]{1,0:T(8,128)(2,1)S(1)} %get-tuple-element.15.weight, f32[256,2048]{1,0:T(8,128)S(1)} %gate.1.gates), custom_call_target="tpu_custom_call" | custom-call | tf_op jit(solution)/shard_map/leave/pallas_call | solution.py:281
Async XLA Ops:
  6.1 35.6 %all-to-all-start = ((bf16[256,8,128]{2,1,0:T(8,128)(2,1)}), bf16[256,8,128]{2,1,0:T(8,128)(2,1)S(1)}, u32[]{:S(2)}, u32[]{:S(2)}) async-start(bf16[256,8,128]{2,1,0:T(8,128)(2,1)} %bitcast.2), calls=%async_computation | async-start | bytes 1048576 | tf_op jit(solution)/shard_map/all_to_all | solution.py:303
  21.8 19.9 %copy-start = (f32[2,256,128]{2,1,0:T(8,128)S(1)}, f32[2,256,128]{2,1,0:T(8,128)}, u32[]{:S(2)}) copy-start(f32[2,256,128]{2,1,0:T(8,128)} %constant.39.clone.twist) | copy-start | bytes 786436
  21.8 19.9 %copy-start.1 = (bf16[512,256]{1,0:T(8,128)(2,1)S(1)}, bf16[512,256]{1,0:T(8,128)(2,1)}, u32[]{:S(2)}) copy-start(bf16[512,256]{1,0:T(8,128)(2,1)} %constant.38.clone.first) | copy-start | bytes 786436
  21.8 19.9 %copy-start.3 = (bf16[128,256]{1,0:T(8,128)(2,1)S(1)}, bf16[128,256]{1,0:T(8,128)(2,1)}, u32[]{:S(2)}) copy-start(bf16[128,256]{1,0:T(8,128)(2,1)} %constant.40.clone.second) | copy-start | bytes 196612
  29.7 40.1 %copy-start.2 = (bf16[256,256]{1,0:T(8,128)(2,1)S(1)}, bf16[256,256]{1,0:T(8,128)(2,1)}, u32[]{:S(2)}) copy-start(bf16[256,256]{1,0:T(8,128)(2,1)} %constant.41.clone.order) | copy-start | bytes 393220
  29.7 40.1 %copy-start.4 = (bf16[128,128]{1,0:T(8,128)(2,1)S(1)}, bf16[128,128]{1,0:T(8,128)(2,1)}, u32[]{:S(2)}) copy-start(bf16[128,128]{1,0:T(8,128)(2,1)} %constant.42.clone.eye) | copy-start | bytes 98308

commit v4 on v3

--- a/solution.py
+++ b/solution.py
@@ -14,13 +14,15 @@
 GROUPS = 8
 GROUP_DIM = 128
 FW = GROUPS * GROUP_DIM
+TWO = 2 * GROUP_DIM
 LENGTH = 32768
 PAIRS = 4
 ROWS = 2 * PAIRS
 NT = (((1,), (1,)), ((), ()))
 F32, BF16 = jnp.float32, jnp.bfloat16
 LEAVE = 4
-ENTER = 256
+EARLY = 1024
+ENTER = 512
 SMALL = pltpu.CompilerParams(vmem_limit_bytes=16 * 2**20)
 
 
@@ -95,19 +97,15 @@
             normed[to, :] = (t * inv * scale[...]).astype(BF16)
             return 0
 
-        lax.fori_loop(0, BLOCK // 16, rows, 0, unroll=4)
+        lax.fori_loop(0, BLOCK // 16, rows, 0, unroll=8)
     save = load(normed, saved, 4 + len(cuts))
     for chunk, cut in zip(chunks, cuts):
         chunk.wait()
         mixed = jnp.dot(normed[...], matrix[:, cut], preferred_element_type=F32).astype(BF16)
-        for q in range(ENTER // GROUP_DIM):
-            turned = lax.dot_general(
-                turn[...],
-                mixed[:, q * GROUP_DIM : (q + 1) * GROUP_DIM],
-                NT,
-                preferred_element_type=F32,
-            )
-            at = slice(cut.start + q * GROUP_DIM, cut.start + (q + 1) * GROUP_DIM)
+        for q in range(ENTER // TWO):
+            part = mixed[:, q * TWO : (q + 1) * TWO]
+            turned = lax.dot_general(turn[...], part, NT, preferred_element_type=F32)
+            at = slice(cut.start + q * TWO, cut.start + (q + 1) * TWO)
             for s in range(SEQS):
                 out[s, at, :] = turned[:, s * BLOCK : (s + 1) * BLOCK].astype(BF16)
     save.wait()
@@ -127,7 +125,7 @@
         scratch_shapes=[
             pltpu.VMEM((SEQS, BLOCK, D), BF16),
             pltpu.VMEM((1, D), F32),
-            pltpu.VMEM((GROUP_DIM, GROUP_DIM), BF16),
+            pltpu.VMEM((TWO, TWO), BF16),
             pltpu.VMEM((SEQS * BLOCK, D), BF16),
             pltpu.VMEM((D, FW), BF16),
             pltpu.SemaphoreType.DMA((5 + FW // ENTER,)),
@@ -138,12 +136,12 @@
         in_hbm(tokens),
         in_hbm(gain.reshape(1, D)),
         in_hbm(weight),
-        in_hbm(jnp.asarray(group_table(), BF16)),
+        in_hbm(jnp.asarray(np.kron(np.eye(2), group_table()), BF16)),
     )
 
 
 def length_body(lone, x, first, twist, second, later, y, kept, wide_in, wide_out, sem):
-    load = pltpu.make_async_copy(later, kept, sem)
+    load = pltpu.make_async_copy(later.at[:, :EARLY], kept, sem)
     load.start()
 
     @pl.when(lone[0] >= 0)
@@ -204,7 +202,7 @@
             pl.BlockSpec(memory_space=pltpu.HBM),
         ],
         out_specs=[vmem, vmem],
-        out_shape=[jax.ShapeDtypeStruct((rows, BLOCK), BF16), pltpu.VMEM(later.shape, BF16)],
+        out_shape=[jax.ShapeDtypeStruct((rows, BLOCK), BF16), pltpu.VMEM((FW, EARLY), BF16)],
         scratch_shapes=[
             pltpu.VMEM((rows, BLOCK), F32),
             pltpu.VMEM((rows, BLOCK), F32),
@@ -247,25 +245,43 @@
     )(in_hbm(normed), in_hbm(weight))
 
 
-def leave_body(z, order, eye, weight, gates, out, spectral, gated, sems):
-    two = 2 * GROUP_DIM
-    for g in range(FW // two):
-        turned = [
-            lax.dot_general(
-                eye[...],
-                z[s * FW + g * two : s * FW + (g + 1) * two, :],
-                NT,
-                preferred_element_type=F32,
-            ).astype(BF16)
-            for s in range(SEQS)
-        ]
-        placed = jnp.dot(jnp.concatenate(turned, axis=0), order[...], preferred_element_type=F32)
-        spectral[:, g * two : (g + 1) * two] = placed.astype(BF16)
+def leave_body(z, order, eye, early, weight, gates, out, late, spectral, gated, loaded, sems):
+    wide = D // LEAVE
+    loads = []
+    for c in range(EARLY // wide, LEAVE):
+        source = weight.at[:, c * wide : (c + 1) * wide]
+        target = late.at[:, c * wide - EARLY : (c + 1) * wide - EARLY]
+        loads.append(pltpu.make_async_copy(source, target, loaded.at[c - EARLY // wide]))
+        loads[-1].start()
+
+    def reorder(g, _):
+        for h in range(2):
+            at = pl.multiple_of((2 * g + h) * TWO, TWO)
+            turned = [
+                lax.dot_general(
+                    eye[...],
+                    z[pl.ds(pl.multiple_of(s * FW + at, TWO), TWO), :],
+                    NT,
+                    preferred_element_type=F32,
+                ).astype(BF16)
+                for s in range(SEQS)
+            ]
+            placed = jnp.dot(
+                jnp.concatenate(turned, axis=0), order[...], preferred_element_type=F32
+            )
+            spectral[:, pl.ds(at, TWO)] = placed.astype(BF16)
+        return 0
+
+    lax.fori_loop(0, FW // TWO // 2, reorder, 0)
     copies = []
-    wide = D // LEAVE
     for c in range(LEAVE):
         at = slice(c * wide, (c + 1) * wide)
-        mapped = jnp.dot(spectral[...], weight[:, at], preferred_element_type=F32)
+        if c * wide < EARLY:
+            part = early[:, at]
+        else:
+            loads[c - EARLY // wide].wait()
+            part = late[:, c * wide - EARLY : (c + 1) * wide - EARLY]
+        mapped = jnp.dot(spectral[...], part, preferred_element_type=F32)
         block = (gates[:, at] * mapped).astype(BF16)
         for s in range(SEQS):
             gated[s, :, at] = block[s * BLOCK : (s + 1) * BLOCK]
@@ -276,16 +292,19 @@
         copy.wait()
 
 
-def leave(z, gates, weight):
+def leave(z, gates, early, weight):
     vmem = pl.BlockSpec(memory_space=pltpu.VMEM)
+    hbm = pl.BlockSpec(memory_space=pltpu.HBM)
     return pl.pallas_call(
         leave_body,
-        in_specs=[vmem] * 5,
-        out_specs=pl.BlockSpec(memory_space=pltpu.HBM),
+        in_specs=[vmem, vmem, vmem, vmem, hbm, vmem],
+        out_specs=hbm,
         out_shape=jax.ShapeDtypeStruct((SEQS, BLOCK, D), BF16),
         scratch_shapes=[
+            pltpu.VMEM((FW, D - EARLY), BF16),
             pltpu.VMEM((SEQS * BLOCK, FW), BF16),
             pltpu.VMEM((SEQS, BLOCK, D), BF16),
+            pltpu.SemaphoreType.DMA((LEAVE,)),
             pltpu.SemaphoreType.DMA((LEAVE,)),
         ],
         compiler_params=SMALL,
@@ -294,7 +313,8 @@
         z,
         jnp.asarray(np.kron(np.eye(2), channel_order()), BF16),
         jnp.asarray(np.eye(GROUP_DIM), BF16),
-        in_vmem(weight),
+        in_vmem(early),
+        in_hbm(weight),
         in_vmem(gates),
     )
 
@@ -310,8 +330,8 @@
     lone = (lax.axis_index(AXES) % (GROUP_DIM // ROWS) == 0).astype(F32).reshape(1)
     arrived = exchange(spectra)
     arrived, gates = lax.optimization_barrier((arrived, gate(normed, gate_weight)))
-    turned, matrix = length_transform(arrived, lone, out_weight)
-    return leave(exchange(turned), gates, matrix)
+    turned, early = length_transform(arrived, lone, out_weight)
+    return leave(exchange(turned), gates, early, out_weight)
 
 
 def solution(mesh):

time: 72.5 us -> 71.3 us (0.983)
  Pallas kernels: 18.6 us -> 17.3 us
    pallas_call x1, Pallas kernels: 6.1 us -> 4.68 us  [enter(): pl.pallas_call(enter_body, in_specs=[hbm] * 4, out_specs=[vmem, hbm], out...]
    pallas_call x1, Pallas kernels: 2.41 us -> 3.18 us  [leave(): pl.pallas_call(leave_body, in_specs=[vmem, vmem, vmem, vmem, hbm, vmem],...]
where the time goes in v4:
time: 71.3 us; the launch traced here: 71 us
  blocking collectives  25.9 us (36%)
  Pallas kernels  17.3 us (24%)
  starting transfers between devices  15.7 us (22%)
  waiting for transfers between devices  12 us (17%)
    all_to_all x1, blocking collectives, exchange(): lax.all_to_all(x.reshape(DEVICES, ROWS, BLOCK), AXES, 0, 0, tiled=True)  25.9 us
    all_to_all x1, starting transfers between devices, exchange(): lax.all_to_all(x.reshape(DEVICES, ROWS, BLOCK), AXES, 0, 0, tiled=True)  15.7 us
    all_to_all x1, waiting for transfers between devices, exchange(): lax.all_to_all(x.reshape(DEVICES, ROWS, BLOCK), AXES, 0, 0, tiled=True)  12 us
    pallas_call x1, Pallas kernels, gate(): pl.pallas_call(gate_body, grid=(steps,), in_specs=[pl.BlockSpec((SEQS * B...  7.85 us
    pallas_call x1, Pallas kernels, enter(): pl.pallas_call(enter_body, in_specs=[hbm] * 4, out_specs=[vmem, hbm], out...  4.68 us
    pallas_call x1, Pallas kernels, leave(): pl.pallas_call(leave_body, in_specs=[vmem, vmem, vmem, vmem, hbm, vmem],...  3.18 us
    pallas_call x1, Pallas kernels, length_transform(): pl.pallas_call(length_body, in_specs=[pl.BlockSpec(memory_space=pltpu.SME...  1.61 us
  transfers between devices with their start and end apart: 1, of which 1 were waited for; matrix products, arithmetic and copies ran while one was open for 0% of the time, Pallas kernels for 11%

profile of v4, /device:TPU:1, one launch (start us, length us, event | category | flops | bytes accessed | tf_op | source)
XLA Modules:
  0.0 71.0 jit_solution(15483700932874782929)
XLA Ops:
  0.0 4.7 %enter.1 = (bf16[2,1024,128]{2,1,0:T(8,128)(2,1)}, bf16[256,2048]{1,0:T(8,128)(2,1)}) custom-call(bf16[2,128,2048]{2,1,0:T(8,128)(2,1)} %tokens.1, f32[1,2048]{1,0:T(1,128)} %bitcast.9, bf16[2048,1024]{1,0:T(8,128)(2,1)} %weight.3, bf16[256,256]{1,0:T(8,128)(2,1)} %constant.37.clone.table), custom_call_target="tpu_custom_call" | custom-call | tf_op jit(solution)/shard_map/enter/pallas_call | solution.py:117
  4.7 15.7 %all-to-all-start = ((bf16[256,8,128]{2,1,0:T(8,128)(2,1)}), bf16[256,8,128]{2,1,0:T(8,128)(2,1)S(1)}, u32[]{:S(2)}, u32[]{:S(2)}) async-start(bf16[256,8,128]{2,1,0:T(8,128)(2,1)} %bitcast.2), calls=%async_computation | async-start | bytes 1048576 | tf_op jit(solution)/shard_map/all_to_all | solution.py:323
  20.4 0.0 copy-start
  20.4 0.0 copy-start.1
  20.4 0.0 copy-start.3
  20.4 7.8 %gate.1.gates = f32[256,2048]{1,0:T(8,128)S(1)} custom-call(bf16[256,2048]{1,0:T(8,128)(2,1)} %get-tuple-element.12.normed, bf16[2048,2048]{1,0:T(8,128)(2,1)} %weight.4), custom_call_target="tpu_custom_call" | custom-call | flops 2147483648 | bytes 8388608 | tf_op jit(solution)/shard_map/gate/pallas_call | solution.py:231
  28.3 0.0 copy-start.2
  28.3 0.0 copy-start.4
  28.3 12.0 %all-to-all-done = bf16[256,8,128]{2,1,0:T(8,128)(2,1)S(1)} async-done(((bf16[256,8,128]{2,1,0:T(8,128)(2,1)}), bf16[256,8,128]{2,1,0:T(8,128)(2,1)S(1)}, u32[]{:S(2)}, u32[]{:S(2)}) %all-to-all-start) | async-done | bytes 524320 | tf_op jit(solution)/shard_map/all_to_all | solution.py:323
  40.3 0.0 copy-done
  40.3 0.0 copy-done.1
  40.3 0.0 copy-done.3
  40.3 1.6 %length.1 = (bf16[2048,128]{1,0:T(8,128)(2,1)S(1)}, bf16[1024,1024]{1,0:T(8,128)(2,1)S(1)}) custom-call(f32[1]{0:T(128)} %bitcast.lone, bf16[2048,128]{1,0:T(8,128)(2,1)S(1)} %bitcast.7, bf16[512,256]{1,0:T(8,128)(2,1)S(1)} %copy-done.1, f32[2,256,128]{2,1,0:T(8,128)S(1)} %copy-done, bf16[128,256]{1,0:T(8,128)(2,1)S(1)} %copy-done.3, bf16[1024,2048]{1,0:T(8,128)(2,1)} %weight.5), custom_call_target="tpu_custom_call" | custom-call | tf_op jit(solution)/shard_map/length/pallas_call | solution.py:194
  41.9 25.9 %all_to_all.10 = bf16[256,8,128]{2,1,0:T(8,128)(2,1)S(1)} all-to-all(bf16[256,8,128]{2,1,0:T(8,128)(2,1)S(1)} %bitcast.8), channel_id=1, replica_groups=mesh['row'=32,'col'=8] {'row','col'}, dimensions={0} | all-to-all | bytes 1048576 | tf_op jit(solution)/shard_map/all_to_all | solution.py:323
  67.8 0.0 copy-done.2
  67.8 0.0 copy-done.4
  67.8 3.2 %leave.1 = bf16[2,128,2048]{2,1,0:T(8,128)(2,1)} custom-call(bf16[2048,128]{1,0:T(8,128)(2,1)S(1)} %bitcast.6, bf16[256,256]{1,0:T(8,128)(2,1)S(1)} %copy-done.2, bf16[128,128]{1,0:T(8,128)(2,1)S(1)} %copy-done.4, bf16[1024,1024]{1,0:T(8,128)(2,1)S(1)} %get-tuple-element.15.early, bf16[1024,2048]{1,0:T(8,128)(2,1)} %weight.5, f32[256,2048]{1,0:T(8,128)S(1)} %gate.1.gates), custom_call_target="tpu_custom_call" | custom-call | tf_op jit(solution)/shard_map/leave/pallas_call | solution.py:298
Async XLA Ops:
  4.7 35.6 %all-to-all-start = ((bf16[256,8,128]{2,1,0:T(8,128)(2,1)}), bf16[256,8,128]{2,1,0:T(8,128)(2,1)S(1)}, u32[]{:S(2)}, u32[]{:S(2)}) async-start(bf16[256,8,128]{2,1,0:T(8,128)(2,1)} %bitcast.2), calls=%async_computation | async-start | bytes 1048576 | tf_op jit(solution)/shard_map/all_to_all | solution.py:323
  20.4 19.9 %copy-start = (f32[2,256,128]{2,1,0:T(8,128)S(1)}, f32[2,256,128]{2,1,0:T(8,128)}, u32[]{:S(2)}) copy-start(f32[2,256,128]{2,1,0:T(8,128)} %constant.39.clone.twist) | copy-start | bytes 786436
  20.4 19.9 %copy-start.1 = (bf16[512,256]{1,0:T(8,128)(2,1)S(1)}, bf16[512,256]{1,0:T(8,128)(2,1)}, u32[]{:S(2)}) copy-start(bf16[512,256]{1,0:T(8,128)(2,1)} %constant.38.clone.first) | copy-start | bytes 786436
  20.4 19.9 %copy-start.3 = (bf16[128,256]{1,0:T(8,128)(2,1)S(1)}, bf16[128,256]{1,0:T(8,128)(2,1)}, u32[]{:S(2)}) copy-start(bf16[128,256]{1,0:T(8,128)(2,1)} %constant.40.clone.second) | copy-start | bytes 196612
  28.3 39.5 %copy-start.2 = (bf16[256,256]{1,0:T(8,128)(2,1)S(1)}, bf16[256,256]{1,0:T(8,128)(2,1)}, u32[]{:S(2)}) copy-start(bf16[256,256]{1,0:T(8,128)(2,1)} %constant.41.clone.order) | copy-start | bytes 393220
  28.3 39.5 %copy-start.4 = (bf16[128,128]{1,0:T(8,128)(2,1)S(1)}, bf16[128,128]{1,0:T(8,128)(2,1)}, u32[]{:S(2)}) copy-start(bf16[128,128]{1,0:T(8,128)(2,1)} %constant.42.clone.eye) | copy-start | bytes 98308

commit v5 on v4

--- a/solution.py
+++ b/solution.py
@@ -11,6 +11,8 @@
 SEQS = 2
 BLOCK = 128
 D = 2048
+LEAVE = 4
+PARTS = D // LEAVE
 GROUPS = 8
 GROUP_DIM = 128
 FW = GROUPS * GROUP_DIM
@@ -20,8 +22,6 @@
 ROWS = 2 * PAIRS
 NT = (((1,), (1,)), ((), ()))
 F32, BF16 = jnp.float32, jnp.bfloat16
-LEAVE = 4
-EARLY = 1024
 ENTER = 512
 SMALL = pltpu.CompilerParams(vmem_limit_bytes=16 * 2**20)
 
@@ -74,7 +74,9 @@
     return np.concatenate([np.cos(angle), -np.sin(angle)], axis=1) / 16
 
 
-def enter_body(tokens, gain, weight, table, out, saved, held, scale, turn, normed, matrix, sems):
+def enter_body(
+    tokens, gain, weight, table, out, saved, held, scale, turn, normed, matrix, spectra, sems
+):
     def load(source, target, at):
         copy = pltpu.make_async_copy(source, target, sems.at[at])
         copy.start()
@@ -98,7 +100,7 @@
             return 0
 
         lax.fori_loop(0, BLOCK // 16, rows, 0, unroll=8)
-    save = load(normed, saved, 4 + len(cuts))
+    saves = [load(normed, saved, 4 + len(cuts))]
     for chunk, cut in zip(chunks, cuts):
         chunk.wait()
         mixed = jnp.dot(normed[...], matrix[:, cut], preferred_element_type=F32).astype(BF16)
@@ -107,19 +109,20 @@
             turned = lax.dot_general(turn[...], part, NT, preferred_element_type=F32)
             at = slice(cut.start + q * TWO, cut.start + (q + 1) * TWO)
             for s in range(SEQS):
-                out[s, at, :] = turned[:, s * BLOCK : (s + 1) * BLOCK].astype(BF16)
-    save.wait()
+                spectra[s, at, :] = turned[:, s * BLOCK : (s + 1) * BLOCK].astype(BF16)
+        saves.append(load(spectra.at[:, cut], out.at[:, cut], 4 + len(cuts) + len(saves)))
+    for save in saves:
+        save.wait()
 
 
 def enter(tokens, gain, weight):
-    vmem = pl.BlockSpec(memory_space=pltpu.VMEM)
     hbm = pl.BlockSpec(memory_space=pltpu.HBM)
     return pl.pallas_call(
         enter_body,
         in_specs=[hbm] * 4,
-        out_specs=[vmem, hbm],
+        out_specs=[hbm, hbm],
         out_shape=[
-            jax.ShapeDtypeStruct((SEQS, FW, BLOCK), BF16),
+            pltpu.HBM((SEQS, FW, BLOCK), BF16),
             pltpu.HBM((SEQS * BLOCK, D), BF16),
         ],
         scratch_shapes=[
@@ -128,7 +131,8 @@
             pltpu.VMEM((TWO, TWO), BF16),
             pltpu.VMEM((SEQS * BLOCK, D), BF16),
             pltpu.VMEM((D, FW), BF16),
-            pltpu.SemaphoreType.DMA((5 + FW // ENTER,)),
+            pltpu.VMEM((SEQS, FW, BLOCK), BF16),
+            pltpu.SemaphoreType.DMA((5 + 2 * (FW // ENTER),)),
         ],
         compiler_params=SMALL,
         name="enter",
@@ -141,7 +145,7 @@
 
 
 def length_body(lone, x, first, twist, second, later, y, kept, wide_in, wide_out, sem):
-    load = pltpu.make_async_copy(later.at[:, :EARLY], kept, sem)
+    load = pltpu.make_async_copy(later.at[:, PARTS : 2 * PARTS], kept, sem)
     load.start()
 
     @pl.when(lone[0] >= 0)
@@ -202,7 +206,7 @@
             pl.BlockSpec(memory_space=pltpu.HBM),
         ],
         out_specs=[vmem, vmem],
-        out_shape=[jax.ShapeDtypeStruct((rows, BLOCK), BF16), pltpu.VMEM((FW, EARLY), BF16)],
+        out_shape=[jax.ShapeDtypeStruct((rows, BLOCK), BF16), pltpu.VMEM((FW, PARTS), BF16)],
         scratch_shapes=[
             pltpu.VMEM((rows, BLOCK), F32),
             pltpu.VMEM((rows, BLOCK), F32),
@@ -220,12 +224,22 @@
     )
 
 
-def gate_body(normed, weight, out):
+def gate_body(normed, weight, later, out, kept, sem):
+    load = pltpu.make_async_copy(later.at[:, :PARTS], kept, sem)
+
+    @pl.when(pl.program_id(0) == 0)
+    def _():
+        load.start()
+
     logits = jnp.dot(normed[...], weight[...], preferred_element_type=F32)
-    out[...] = jax.nn.sigmoid(logits)
-
-
-def gate(normed, weight):
+    out[...] = jax.nn.sigmoid(logits).astype(BF16)
+
+    @pl.when(pl.program_id(0) == pl.num_programs(0) - 1)
+    def _():
+        load.wait()
+
+
+def gate(normed, weight, later):
     steps = 8
     wide = D // steps
     return pl.pallas_call(
@@ -234,33 +248,38 @@
         in_specs=[
             pl.BlockSpec((SEQS * BLOCK, D), lambda j: (0, 0)),
             pl.BlockSpec((D, wide), lambda j: (0, j)),
-        ],
-        out_specs=pl.BlockSpec((SEQS * BLOCK, wide), lambda j: (0, j)),
-        out_shape=pltpu.VMEM((SEQS * BLOCK, D), F32),
+            pl.BlockSpec(memory_space=pltpu.HBM),
+        ],
+        out_specs=[
+            pl.BlockSpec((SEQS * BLOCK, wide), lambda j: (0, j)),
+            pl.BlockSpec(memory_space=pltpu.VMEM),
+        ],
+        out_shape=[pltpu.VMEM((SEQS * BLOCK, D), BF16), pltpu.VMEM((FW, PARTS), BF16)],
+        scratch_shapes=[pltpu.SemaphoreType.DMA],
         cost_estimate=pl.CostEstimate(
             flops=2 * SEQS * BLOCK * D * D, transcendentals=SEQS * BLOCK * D, bytes_accessed=2 * D * D
         ),
         compiler_params=SMALL,
         name="gate",
-    )(in_hbm(normed), in_hbm(weight))
-
-
-def leave_body(z, order, eye, early, weight, gates, out, late, spectral, gated, loaded, sems):
-    wide = D // LEAVE
+    )(in_hbm(normed), in_hbm(weight), in_hbm(later))
+
+
+def leave_body(
+    lone, z, order, eye, part_0, part_1, weight, gates, out, late, spectral, gated, loaded, sems
+):
     loads = []
-    for c in range(EARLY // wide, LEAVE):
-        source = weight.at[:, c * wide : (c + 1) * wide]
-        target = late.at[:, c * wide - EARLY : (c + 1) * wide - EARLY]
-        loads.append(pltpu.make_async_copy(source, target, loaded.at[c - EARLY // wide]))
+    for c in range(2, LEAVE):
+        source = weight.at[:, c * PARTS : (c + 1) * PARTS]
+        loads.append(pltpu.make_async_copy(source, late.at[c - 2], loaded.at[c - 2]))
         loads[-1].start()
 
-    def reorder(g, _):
-        for h in range(2):
-            at = pl.multiple_of((2 * g + h) * TWO, TWO)
+    @pl.when(lone[0] >= 0)
+    def _():
+        for g in range(FW // TWO):
             turned = [
                 lax.dot_general(
                     eye[...],
-                    z[pl.ds(pl.multiple_of(s * FW + at, TWO), TWO), :],
+                    z[s * FW + g * TWO : s * FW + (g + 1) * TWO, :],
                     NT,
                     preferred_element_type=F32,
                 ).astype(BF16)
@@ -269,20 +288,16 @@
             placed = jnp.dot(
                 jnp.concatenate(turned, axis=0), order[...], preferred_element_type=F32
             )
-            spectral[:, pl.ds(at, TWO)] = placed.astype(BF16)
-        return 0
-
-    lax.fori_loop(0, FW // TWO // 2, reorder, 0)
+            spectral[:, g * TWO : (g + 1) * TWO] = placed.astype(BF16)
+
     copies = []
     for c in range(LEAVE):
-        at = slice(c * wide, (c + 1) * wide)
-        if c * wide < EARLY:
-            part = early[:, at]
-        else:
-            loads[c - EARLY // wide].wait()
-            part = late[:, c * wide - EARLY : (c + 1) * wide - EARLY]
+        at = slice(c * PARTS, (c + 1) * PARTS)
+        if c >= 2:
+            loads[c - 2].wait()
+        part = (part_0, part_1)[c][...] if c < 2 else late[c - 2]
         mapped = jnp.dot(spectral[...], part, preferred_element_type=F32)
-        block = (gates[:, at] * mapped).astype(BF16)
+        block = (gates[:, at].astype(F32) * mapped).astype(BF16)
         for s in range(SEQS):
             gated[s, :, at] = block[s * BLOCK : (s + 1) * BLOCK]
         copy = pltpu.make_async_copy(gated.at[:, :, at], out.at[:, :, at], sems.at[c])
@@ -292,16 +307,16 @@
         copy.wait()
 
 
-def leave(z, gates, early, weight):
+def leave(z, gates, part_0, part_1, weight, lone):
     vmem = pl.BlockSpec(memory_space=pltpu.VMEM)
     hbm = pl.BlockSpec(memory_space=pltpu.HBM)
     return pl.pallas_call(
         leave_body,
-        in_specs=[vmem, vmem, vmem, vmem, hbm, vmem],
+        in_specs=[pl.BlockSpec(memory_space=pltpu.SMEM), vmem, vmem, vmem, vmem, vmem, hbm, vmem],
         out_specs=hbm,
         out_shape=jax.ShapeDtypeStruct((SEQS, BLOCK, D), BF16),
         scratch_shapes=[
-            pltpu.VMEM((FW, D - EARLY), BF16),
+            pltpu.VMEM((LEAVE - 2, FW, PARTS), BF16),
             pltpu.VMEM((SEQS * BLOCK, FW), BF16),
             pltpu.VMEM((SEQS, BLOCK, D), BF16),
             pltpu.SemaphoreType.DMA((LEAVE,)),
@@ -310,10 +325,12 @@
         compiler_params=SMALL,
         name="leave",
     )(
+        lone,
         z,
         jnp.asarray(np.kron(np.eye(2), channel_order()), BF16),
         jnp.asarray(np.eye(GROUP_DIM), BF16),
-        in_vmem(early),
+        in_vmem(part_0),
+        in_vmem(part_1),
         in_hbm(weight),
         in_vmem(gates),
     )
@@ -329,9 +346,11 @@
     spectra, normed = enter(tokens, norm_gain, mix_weight)
     lone = (lax.axis_index(AXES) % (GROUP_DIM // ROWS) == 0).astype(F32).reshape(1)
     arrived = exchange(spectra)
-    arrived, gates = lax.optimization_barrier((arrived, gate(normed, gate_weight)))
-    turned, early = length_transform(arrived, lone, out_weight)
-    return leave(exchange(turned), gates, early, out_weight)
+    arrived, (gates, part_0) = lax.optimization_barrier(
+        (arrived, gate(normed, gate_weight, out_weight))
+    )
+    turned, part_1 = length_transform(arrived, lone, out_weight)
+    return leave(exchange(turned), gates, part_0, part_1, out_weight, lone)
 
 
 def solution(mesh):

time: 71.3 us -> 70.6 us (level)
  no operation moved by 1% of the time
where the time goes in v5:
time: 70.6 us; the launch traced here: 70.3 us
  blocking collectives  25.9 us (37%)
  Pallas kernels  16.7 us (24%)
  starting transfers between devices  15.7 us (22%)
  waiting for transfers between devices  11.9 us (17%)
    all_to_all x1, blocking collectives, exchange(): lax.all_to_all(x.reshape(DEVICES, ROWS, BLOCK), AXES, 0, 0, tiled=True)  25.9 us
    all_to_all x1, starting transfers between devices, exchange(): lax.all_to_all(x.reshape(DEVICES, ROWS, BLOCK), AXES, 0, 0, tiled=True)  15.7 us
    all_to_all x1, waiting for transfers between devices, exchange(): lax.all_to_all(x.reshape(DEVICES, ROWS, BLOCK), AXES, 0, 0, tiled=True)  11.9 us
    pallas_call x1, Pallas kernels, gate(): pl.pallas_call(gate_body, grid=(steps,), in_specs=[pl.BlockSpec((SEQS * B...  7.97 us
    pallas_call x1, Pallas kernels, enter(): pl.pallas_call(enter_body, in_specs=[hbm] * 4, out_specs=[hbm, hbm], out_...  4.6 us
    pallas_call x1, Pallas kernels, leave(): pl.pallas_call(leave_body, in_specs=[pl.BlockSpec(memory_space=pltpu.SMEM...  2.9 us
  transfers between devices with their start and end apart: 1, of which 1 were waited for; matrix products, arithmetic and copies ran while one was open for 0% of the time, Pallas kernels for 11%

profile of v5, /device:TPU:1, one launch (start us, length us, event | category | flops | bytes accessed | tf_op | source)
XLA Modules:
  0.0 70.3 jit_solution(1087485859938685440)
XLA Ops:
  0.0 4.6 %enter.1 = (bf16[2,1024,128]{2,1,0:T(8,128)(2,1)}, bf16[256,2048]{1,0:T(8,128)(2,1)}) custom-call(bf16[2,128,2048]{2,1,0:T(8,128)(2,1)} %tokens.1, f32[1,2048]{1,0:T(1,128)} %bitcast.10, bf16[2048,1024]{1,0:T(8,128)(2,1)} %weight.3, bf16[256,256]{1,0:T(8,128)(2,1)} %constant.37.clone.table), custom_call_target="tpu_custom_call" | custom-call | tf_op jit(solution)/shard_map/enter/pallas_call | solution.py:120
  4.6 15.7 %all-to-all-start = ((bf16[256,8,128]{2,1,0:T(8,128)(2,1)}), bf16[256,8,128]{2,1,0:T(8,128)(2,1)S(1)}, u32[]{:S(2)}, u32[]{:S(2)}) async-start(bf16[256,8,128]{2,1,0:T(8,128)(2,1)} %bitcast.9), calls=%async_computation | async-start | bytes 1048576 | tf_op jit(solution)/shard_map/all_to_all | solution.py:340
  20.3 0.0 copy-start
  20.3 0.0 copy-start.1
  20.3 0.0 copy-start.3
  20.3 8.0 %gate.1 = (bf16[256,2048]{1,0:T(8,128)(2,1)S(1)}, bf16[1024,512]{1,0:T(8,128)(2,1)S(1)}) custom-call(bf16[256,2048]{1,0:T(8,128)(2,1)} %get-tuple-element.15.normed, bf16[2048,2048]{1,0:T(8,128)(2,1)} %weight.4, bf16[1024,2048]{1,0:T(8,128)(2,1)} %weight.5), custom_call_target="tpu_custom_call" | custom-call | flops 2147483648 | bytes 8388608 | tf_op jit(solution)/shard_map/gate/pallas_call | solution.py:245
  28.3 0.0 copy-start.2
  28.3 0.0 copy-start.4
  28.3 11.9 %all-to-all-done = bf16[256,8,128]{2,1,0:T(8,128)(2,1)S(1)} async-done(((bf16[256,8,128]{2,1,0:T(8,128)(2,1)}), bf16[256,8,128]{2,1,0:T(8,128)(2,1)S(1)}, u32[]{:S(2)}, u32[]{:S(2)}) %all-to-all-start) | async-done | bytes 524320 | tf_op jit(solution)/shard_map/all_to_all | solution.py:340
  40.2 0.0 copy-done
  40.2 0.0 copy-done.1
  40.2 0.0 copy-done.3
  40.2 1.2 %length.1 = (bf16[2048,128]{1,0:T(8,128)(2,1)S(1)}, bf16[1024,512]{1,0:T(8,128)(2,1)S(1)}) custom-call(f32[1]{0:T(128)} %bitcast.lone, bf16[2048,128]{1,0:T(8,128)(2,1)S(1)} %bitcast.7, bf16[512,256]{1,0:T(8,128)(2,1)S(1)} %copy-done.1, f32[2,256,128]{2,1,0:T(8,128)S(1)} %copy-done, bf16[128,256]{1,0:T(8,128)(2,1)S(1)} %copy-done.3, bf16[1024,2048]{1,0:T(8,128)(2,1)} %weight.5), custom_call_target="tpu_custom_call" | custom-call | tf_op jit(solution)/shard_map/length/pallas_call | solution.py:198
  41.5 25.9 %all_to_all.10 = bf16[256,8,128]{2,1,0:T(8,128)(2,1)S(1)} all-to-all(bf16[256,8,128]{2,1,0:T(8,128)(2,1)S(1)} %bitcast.8), channel_id=1, replica_groups=mesh['row'=32,'col'=8] {'row','col'}, dimensions={0} | all-to-all | bytes 1048576 | tf_op jit(solution)/shard_map/all_to_all | solution.py:340
  67.3 0.0 copy-done.2
  67.3 0.0 copy-done.4
  67.3 2.9 %leave.1 = bf16[2,128,2048]{2,1,0:T(8,128)(2,1)} custom-call(f32[1]{0:T(128)} %bitcast.lone, bf16[2048,128]{1,0:T(8,128)(2,1)S(1)} %bitcast.6, bf16[256,256]{1,0:T(8,128)(2,1)S(1)} %copy-done.2, bf16[128,128]{1,0:T(8,128)(2,1)S(1)} %copy-done.4, bf16[1024,512]{1,0:T(8,128)(2,1)S(1)} %get-tuple-element.20.part_0, ...), custom_call_target="tpu_custom_call" | custom-call | tf_op jit(solution)/shard_map/leave/pallas_call | solution.py:313
Async XLA Ops:
  4.6 35.6 %all-to-all-start = ((bf16[256,8,128]{2,1,0:T(8,128)(2,1)}), bf16[256,8,128]{2,1,0:T(8,128)(2,1)S(1)}, u32[]{:S(2)}, u32[]{:S(2)}) async-start(bf16[256,8,128]{2,1,0:T(8,128)(2,1)} %bitcast.9), calls=%async_computation | async-start | bytes 1048576 | tf_op jit(solution)/shard_map/all_to_all | solution.py:340
  20.3 19.9 %copy-start = (f32[2,256,128]{2,1,0:T(8,128)S(1)}, f32[2,256,128]{2,1,0:T(8,128)}, u32[]{:S(2)}) copy-start(f32[2,256,128]{2,1,0:T(8,128)} %constant.39.clone.twist) | copy-start | bytes 786436
  20.3 19.9 %copy-start.1 = (bf16[512,256]{1,0:T(8,128)(2,1)S(1)}, bf16[512,256]{1,0:T(8,128)(2,1)}, u32[]{:S(2)}) copy-start(bf16[512,256]{1,0:T(8,128)(2,1)} %constant.38.clone.first) | copy-start | bytes 786436
  20.3 19.9 %copy-start.3 = (bf16[128,256]{1,0:T(8,128)(2,1)S(1)}, bf16[128,256]{1,0:T(8,128)(2,1)}, u32[]{:S(2)}) copy-start(bf16[128,256]{1,0:T(8,128)(2,1)} %constant.40.clone.second) | copy-start | bytes 196612
  28.3 39.0 %copy-start.2 = (bf16[256,256]{1,0:T(8,128)(2,1)S(1)}, bf16[256,256]{1,0:T(8,128)(2,1)}, u32[]{:S(2)}) copy-start(bf16[256,256]{1,0:T(8,128)(2,1)} %constant.41.clone.order) | copy-start | bytes 393220
  28.3 39.0 %copy-start.4 = (bf16[128,128]{1,0:T(8,128)(2,1)S(1)}, bf16[128,128]{1,0:T(8,128)(2,1)}, u32[]{:S(2)}) copy-start(bf16[128,128]{1,0:T(8,128)(2,1)} %constant.42.clone.eye) | copy-start | bytes 98308

commit v6 on v5

--- a/solution.py
+++ b/solution.py
@@ -21,6 +21,7 @@
 PAIRS = 4
 ROWS = 2 * PAIRS
 NT = (((1,), (1,)), ((), ()))
+TN = (((0,), (0,)), ((), ()))
 F32, BF16 = jnp.float32, jnp.bfloat16
 ENTER = 512
 SMALL = pltpu.CompilerParams(vmem_limit_bytes=16 * 2**20)
@@ -100,9 +101,11 @@
             return 0
 
         lax.fori_loop(0, BLOCK // 16, rows, 0, unroll=8)
-    saves = [load(normed, saved, 4 + len(cuts))]
+    saves = []
     for chunk, cut in zip(chunks, cuts):
         chunk.wait()
+        if cut.stop == FW:
+            saves.append(load(normed, saved, 4 + len(cuts) + len(saves)))
         mixed = jnp.dot(normed[...], matrix[:, cut], preferred_element_type=F32).astype(BF16)
         for q in range(ENTER // TWO):
             part = mixed[:, q * TWO : (q + 1) * TWO]
@@ -265,7 +268,7 @@
 
 
 def leave_body(
-    lone, z, order, eye, part_0, part_1, weight, gates, out, late, spectral, gated, loaded, sems
+    lone, z, order, part_0, part_1, weight, gates, out, late, spectral, gated, loaded, sems
 ):
     loads = []
     for c in range(2, LEAVE):
@@ -276,19 +279,10 @@
     @pl.when(lone[0] >= 0)
     def _():
         for g in range(FW // TWO):
-            turned = [
-                lax.dot_general(
-                    eye[...],
-                    z[s * FW + g * TWO : s * FW + (g + 1) * TWO, :],
-                    NT,
-                    preferred_element_type=F32,
-                ).astype(BF16)
-                for s in range(SEQS)
-            ]
-            placed = jnp.dot(
-                jnp.concatenate(turned, axis=0), order[...], preferred_element_type=F32
-            )
-            spectral[:, g * TWO : (g + 1) * TWO] = placed.astype(BF16)
+            for s in range(SEQS):
+                rows = z[s * FW + g * TWO : s * FW + (g + 1) * TWO, :]
+                placed = lax.dot_general(rows, order[...], TN, preferred_element_type=F32)
+                spectral[s * BLOCK : (s + 1) * BLOCK, g * TWO : (g + 1) * TWO] = placed.astype(BF16)
 
     copies = []
     for c in range(LEAVE):
@@ -312,7 +306,7 @@
     hbm = pl.BlockSpec(memory_space=pltpu.HBM)
     return pl.pallas_call(
         leave_body,
-        in_specs=[pl.BlockSpec(memory_space=pltpu.SMEM), vmem, vmem, vmem, vmem, vmem, hbm, vmem],
+        in_specs=[pl.BlockSpec(memory_space=pltpu.SMEM), vmem, vmem, vmem, vmem, hbm, vmem],
         out_specs=hbm,
         out_shape=jax.ShapeDtypeStruct((SEQS, BLOCK, D), BF16),
         scratch_shapes=[
@@ -328,7 +322,6 @@
         lone,
         z,
         jnp.asarray(np.kron(np.eye(2), channel_order()), BF16),
-        jnp.asarray(np.eye(GROUP_DIM), BF16),
         in_vmem(part_0),
         in_vmem(part_1),
         in_hbm(weight),

time: 70.6 us -> 70.5 us (level)
  no operation moved by 1% of the time
where the time goes in v6:
time: 70.5 us; the launch traced here: 70.2 us
  blocking collectives  25.9 us (37%)
  Pallas kernels  16.7 us (24%)
  starting transfers between devices  15.7 us (22%)
  waiting for transfers between devices  11.9 us (17%)
    all_to_all x1, blocking collectives, exchange(): lax.all_to_all(x.reshape(DEVICES, ROWS, BLOCK), AXES, 0, 0, tiled=True)  25.9 us
    all_to_all x1, starting transfers between devices, exchange(): lax.all_to_all(x.reshape(DEVICES, ROWS, BLOCK), AXES, 0, 0, tiled=True)  15.7 us
    all_to_all x1, waiting for transfers between devices, exchange(): lax.all_to_all(x.reshape(DEVICES, ROWS, BLOCK), AXES, 0, 0, tiled=True)  11.9 us
    pallas_call x1, Pallas kernels, gate(): pl.pallas_call(gate_body, grid=(steps,), in_specs=[pl.BlockSpec((SEQS * B...  7.97 us
    pallas_call x1, Pallas kernels, enter(): pl.pallas_call(enter_body, in_specs=[hbm] * 4, out_specs=[hbm, hbm], out_...  4.59 us
    pallas_call x1, Pallas kernels, leave(): pl.pallas_call(leave_body, in_specs=[pl.BlockSpec(memory_space=pltpu.SMEM...  2.87 us
  transfers between devices with their start and end apart: 1, of which 1 were waited for; matrix products, arithmetic and copies ran while one was open for 0% of the time, Pallas kernels for 11%

profile of v6, /device:TPU:1, one launch (start us, length us, event | category | flops | bytes accessed | tf_op | source)
XLA Modules:
  0.0 70.2 jit_solution(17470192645003815635)
XLA Ops:
  0.0 4.6 %enter.1 = (bf16[2,1024,128]{2,1,0:T(8,128)(2,1)}, bf16[256,2048]{1,0:T(8,128)(2,1)}) custom-call(bf16[2,128,2048]{2,1,0:T(8,128)(2,1)} %tokens.1, f32[1,2048]{1,0:T(1,128)} %bitcast.10, bf16[2048,1024]{1,0:T(8,128)(2,1)} %weight.3, bf16[256,256]{1,0:T(8,128)(2,1)} %constant.35.clone.table), custom_call_target="tpu_custom_call" | custom-call | tf_op jit(solution)/shard_map/enter/pallas_call | solution.py:123
  4.6 15.7 %all-to-all-start = ((bf16[256,8,128]{2,1,0:T(8,128)(2,1)}), bf16[256,8,128]{2,1,0:T(8,128)(2,1)S(1)}, u32[]{:S(2)}, u32[]{:S(2)}) async-start(bf16[256,8,128]{2,1,0:T(8,128)(2,1)} %bitcast.9), calls=%async_computation | async-start | bytes 1048576 | tf_op jit(solution)/shard_map/all_to_all | solution.py:333
  20.3 0.0 copy-start
  20.3 0.0 copy-start.1
  20.3 0.0 copy-start.3
  20.3 8.0 %gate.1 = (bf16[256,2048]{1,0:T(8,128)(2,1)S(1)}, bf16[1024,512]{1,0:T(8,128)(2,1)S(1)}) custom-call(bf16[256,2048]{1,0:T(8,128)(2,1)} %get-tuple-element.15.normed, bf16[2048,2048]{1,0:T(8,128)(2,1)} %weight.4, bf16[1024,2048]{1,0:T(8,128)(2,1)} %weight.5), custom_call_target="tpu_custom_call" | custom-call | flops 2147483648 | bytes 8388608 | tf_op jit(solution)/shard_map/gate/pallas_call | solution.py:248
  28.3 0.0 copy-start.2
  28.3 11.9 %all-to-all-done = bf16[256,8,128]{2,1,0:T(8,128)(2,1)S(1)} async-done(((bf16[256,8,128]{2,1,0:T(8,128)(2,1)}), bf16[256,8,128]{2,1,0:T(8,128)(2,1)S(1)}, u32[]{:S(2)}, u32[]{:S(2)}) %all-to-all-start) | async-done | bytes 524320 | tf_op jit(solution)/shard_map/all_to_all | solution.py:333
  40.2 0.0 copy-done
  40.2 0.0 copy-done.1
  40.2 0.0 copy-done.3
  40.2 1.2 %length.1 = (bf16[2048,128]{1,0:T(8,128)(2,1)S(1)}, bf16[1024,512]{1,0:T(8,128)(2,1)S(1)}) custom-call(f32[1]{0:T(128)} %bitcast.lone, bf16[2048,128]{1,0:T(8,128)(2,1)S(1)} %bitcast.7, bf16[512,256]{1,0:T(8,128)(2,1)S(1)} %copy-done.1, f32[2,256,128]{2,1,0:T(8,128)S(1)} %copy-done, bf16[128,256]{1,0:T(8,128)(2,1)S(1)} %copy-done.3, bf16[1024,2048]{1,0:T(8,128)(2,1)} %weight.5), custom_call_target="tpu_custom_call" | custom-call | tf_op jit(solution)/shard_map/length/pallas_call | solution.py:201
  41.5 25.9 %all_to_all.10 = bf16[256,8,128]{2,1,0:T(8,128)(2,1)S(1)} all-to-all(bf16[256,8,128]{2,1,0:T(8,128)(2,1)S(1)} %bitcast.8), channel_id=1, replica_groups=mesh['row'=32,'col'=8] {'row','col'}, dimensions={0} | all-to-all | bytes 1048576 | tf_op jit(solution)/shard_map/all_to_all | solution.py:333
  67.3 0.0 copy-done.2
  67.3 2.9 %leave.1 = bf16[2,128,2048]{2,1,0:T(8,128)(2,1)} custom-call(f32[1]{0:T(128)} %bitcast.lone, bf16[2048,128]{1,0:T(8,128)(2,1)S(1)} %bitcast.6, bf16[256,256]{1,0:T(8,128)(2,1)S(1)} %copy-done.2, bf16[1024,512]{1,0:T(8,128)(2,1)S(1)} %get-tuple-element.20.part_0, bf16[1024,512]{1,0:T(8,128)(2,1)S(1)} %get-tuple-element.21.part_1, bf16[1024,2048]{1,0:T(8,128)(2,1)} %weight.5, ...), custom_call_target="tpu_custom_call" | custom-call | tf_op jit(solution)/shard_map/leave/pallas_call | solution.py:307
Async XLA Ops:
  4.6 35.6 %all-to-all-start = ((bf16[256,8,128]{2,1,0:T(8,128)(2,1)}), bf16[256,8,128]{2,1,0:T(8,128)(2,1)S(1)}, u32[]{:S(2)}, u32[]{:S(2)}) async-start(bf16[256,8,128]{2,1,0:T(8,128)(2,1)} %bitcast.9), calls=%async_computation | async-start | bytes 1048576 | tf_op jit(solution)/shard_map/all_to_all | solution.py:333
  20.3 19.9 %copy-start = (f32[2,256,128]{2,1,0:T(8,128)S(1)}, f32[2,256,128]{2,1,0:T(8,128)}, u32[]{:S(2)}) copy-start(f32[2,256,128]{2,1,0:T(8,128)} %constant.37.clone.twist) | copy-start | bytes 786436
  20.3 19.9 %copy-start.1 = (bf16[512,256]{1,0:T(8,128)(2,1)S(1)}, bf16[512,256]{1,0:T(8,128)(2,1)}, u32[]{:S(2)}) copy-start(bf16[512,256]{1,0:T(8,128)(2,1)} %constant.36.clone.first) | copy-start | bytes 786436
  20.3 19.9 %copy-start.3 = (bf16[128,256]{1,0:T(8,128)(2,1)S(1)}, bf16[128,256]{1,0:T(8,128)(2,1)}, u32[]{:S(2)}) copy-start(bf16[128,256]{1,0:T(8,128)(2,1)} %constant.38.clone.second) | copy-start | bytes 196612
  28.3 39.0 %copy-start.2 = (bf16[256,256]{1,0:T(8,128)(2,1)S(1)}, bf16[256,256]{1,0:T(8,128)(2,1)}, u32[]{:S(2)}) copy-start(bf16[256,256]{1,0:T(8,128)(2,1)} %constant.39.clone.order) | copy-start | bytes 393220

commit v7 on v6

--- a/solution.py
+++ b/solution.py
@@ -227,38 +227,48 @@
     )
 
 
-def gate_body(normed, weight, later, out, kept, sem):
-    load = pltpu.make_async_copy(later.at[:, :PARTS], kept, sem)
+LATE = [slice(c * PARTS, (c + 1) * PARTS) for c in range(2, LEAVE)]
+
+
+def gate_body(normed, weight, later, out, kept, *refs):
+    loads = [pltpu.make_async_copy(later.at[:, :PARTS], kept, refs[-1].at[0])]
+    for c, cut in enumerate(LATE):
+        loads.append(pltpu.make_async_copy(later.at[:, cut], refs[c], refs[-1].at[1 + c]))
 
     @pl.when(pl.program_id(0) == 0)
     def _():
-        load.start()
+        for load in loads:
+            load.start()
 
     logits = jnp.dot(normed[...], weight[...], preferred_element_type=F32)
     out[...] = jax.nn.sigmoid(logits).astype(BF16)
 
     @pl.when(pl.program_id(0) == pl.num_programs(0) - 1)
     def _():
-        load.wait()
+        for load in loads:
+            load.wait()
 
 
 def gate(normed, weight, later):
     steps = 8
     wide = D // steps
+    hbm = pl.BlockSpec(memory_space=pltpu.HBM)
     return pl.pallas_call(
         gate_body,
         grid=(steps,),
         in_specs=[
             pl.BlockSpec((SEQS * BLOCK, D), lambda j: (0, 0)),
             pl.BlockSpec((D, wide), lambda j: (0, j)),
-            pl.BlockSpec(memory_space=pltpu.HBM),
+            hbm,
         ],
         out_specs=[
             pl.BlockSpec((SEQS * BLOCK, wide), lambda j: (0, j)),
             pl.BlockSpec(memory_space=pltpu.VMEM),
-        ],
-        out_shape=[pltpu.VMEM((SEQS * BLOCK, D), BF16), pltpu.VMEM((FW, PARTS), BF16)],
-        scratch_shapes=[pltpu.SemaphoreType.DMA],
+        ]
+        + [hbm] * len(LATE),
+        out_shape=[pltpu.VMEM((SEQS * BLOCK, D), BF16), pltpu.VMEM((FW, PARTS), BF16)]
+        + [pltpu.HBM((FW, PARTS), BF16)] * len(LATE),
+        scratch_shapes=[pltpu.SemaphoreType.DMA((1 + len(LATE),))],
         cost_estimate=pl.CostEstimate(
             flops=2 * SEQS * BLOCK * D * D, transcendentals=SEQS * BLOCK * D, bytes_accessed=2 * D * D
         ),
@@ -267,30 +277,17 @@
     )(in_hbm(normed), in_hbm(weight), in_hbm(later))
 
 
-def leave_body(
-    lone, z, order, part_0, part_1, weight, gates, out, late, spectral, gated, loaded, sems
-):
-    loads = []
-    for c in range(2, LEAVE):
-        source = weight.at[:, c * PARTS : (c + 1) * PARTS]
-        loads.append(pltpu.make_async_copy(source, late.at[c - 2], loaded.at[c - 2]))
-        loads[-1].start()
-
-    @pl.when(lone[0] >= 0)
-    def _():
-        for g in range(FW // TWO):
-            for s in range(SEQS):
-                rows = z[s * FW + g * TWO : s * FW + (g + 1) * TWO, :]
-                placed = lax.dot_general(rows, order[...], TN, preferred_element_type=F32)
-                spectral[s * BLOCK : (s + 1) * BLOCK, g * TWO : (g + 1) * TWO] = placed.astype(BF16)
-
+def leave_body(z, order, gates, *refs):
+    parts, (out, spectral, gated, sems) = refs[:LEAVE], refs[LEAVE:]
+    for g in range(FW // TWO):
+        for s in range(SEQS):
+            rows = z[s * FW + g * TWO : s * FW + (g + 1) * TWO, :]
+            placed = lax.dot_general(rows, order[...], TN, preferred_element_type=F32)
+            spectral[s * BLOCK : (s + 1) * BLOCK, g * TWO : (g + 1) * TWO] = placed.astype(BF16)
     copies = []
     for c in range(LEAVE):
         at = slice(c * PARTS, (c + 1) * PARTS)
-        if c >= 2:
-            loads[c - 2].wait()
-        part = (part_0, part_1)[c][...] if c < 2 else late[c - 2]
-        mapped = jnp.dot(spectral[...], part, preferred_element_type=F32)
+        mapped = jnp.dot(spectral[...], parts[c][...], preferred_element_type=F32)
         block = (gates[:, at].astype(F32) * mapped).astype(BF16)
         for s in range(SEQS):
             gated[s, :, at] = block[s * BLOCK : (s + 1) * BLOCK]
@@ -301,31 +298,24 @@
         copy.wait()
 
 
-def leave(z, gates, part_0, part_1, weight, lone):
+def leave(z, gates, *parts):
     vmem = pl.BlockSpec(memory_space=pltpu.VMEM)
-    hbm = pl.BlockSpec(memory_space=pltpu.HBM)
     return pl.pallas_call(
         leave_body,
-        in_specs=[pl.BlockSpec(memory_space=pltpu.SMEM), vmem, vmem, vmem, vmem, hbm, vmem],
-        out_specs=hbm,
+        in_specs=[vmem] * (3 + len(parts)),
+        out_specs=pl.BlockSpec(memory_space=pltpu.HBM),
         out_shape=jax.ShapeDtypeStruct((SEQS, BLOCK, D), BF16),
         scratch_shapes=[
-            pltpu.VMEM((LEAVE - 2, FW, PARTS), BF16),
             pltpu.VMEM((SEQS * BLOCK, FW), BF16),
             pltpu.VMEM((SEQS, BLOCK, D), BF16),
             pltpu.SemaphoreType.DMA((LEAVE,)),
-            pltpu.SemaphoreType.DMA((LEAVE,)),
         ],
         compiler_params=SMALL,
         name="leave",
     )(
-        lone,
         z,
         jnp.asarray(np.kron(np.eye(2), channel_order()), BF16),
-        in_vmem(part_0),
-        in_vmem(part_1),
-        in_hbm(weight),
-        in_vmem(gates),
+        *(in_vmem(held) for held in (gates, *parts)),
     )
 
 
@@ -339,11 +329,11 @@
     spectra, normed = enter(tokens, norm_gain, mix_weight)
     lone = (lax.axis_index(AXES) % (GROUP_DIM // ROWS) == 0).astype(F32).reshape(1)
     arrived = exchange(spectra)
-    arrived, (gates, part_0) = lax.optimization_barrier(
+    arrived, (gates, part_0, *late) = lax.optimization_barrier(
         (arrived, gate(normed, gate_weight, out_weight))
     )
     turned, part_1 = length_transform(arrived, lone, out_weight)
-    return leave(exchange(turned), gates, part_0, part_1, out_weight, lone)
+    return leave(exchange(turned), gates, part_0, part_1, *late)
 
 
 def solution(mesh):

time: 70.5 us -> 124 us (1.76)
  Pallas kernels: 16.7 us -> 74.5 us
  waiting for transfers between devices: 11.9 us -> 0.01 us
  blocking collectives: 25.9 us -> 33.5 us
    pallas_call x1, Pallas kernels: 7.97 us -> 66.3 us  [gate(): pl.pallas_call(gate_body, grid=(steps,), in_specs=[pl.BlockSpec((SEQS * B...]
    all_to_all x1, waiting for transfers between devices: 11.9 us -> 0.01 us  [exchange(): lax.all_to_all(x.reshape(DEVICES, ROWS, BLOCK), AXES, 0, 0, tiled=True)]
    all_to_all x1, blocking collectives: 25.9 us -> 33.5 us  [exchange(): lax.all_to_all(x.reshape(DEVICES, ROWS, BLOCK), AXES, 0, 0, tiled=True)]
  transfers between devices with their start and end apart: 1 -> 1, of which waited for: 1 -> 0; matrix products, arithmetic and copies ran while one was open for 0% -> 0% of each run, Pallas kernels for 11% -> 54%
where the time goes in v7:
time: 124 us
  Pallas kernels  74.5 us (60%)
  blocking collectives  33.5 us (27%)
  starting transfers between devices  15.7 us (13%)
    pallas_call x1, Pallas kernels, gate(): pl.pallas_call(gate_body, grid=(steps,), in_specs=[pl.BlockSpec((SEQS * B...  66.3 us
    all_to_all x1, blocking collectives, exchange(): lax.all_to_all(x.reshape(DEVICES, ROWS, BLOCK), AXES, 0, 0, tiled=True)  33.5 us
    all_to_all x1, starting transfers between devices, exchange(): lax.all_to_all(x.reshape(DEVICES, ROWS, BLOCK), AXES, 0, 0, tiled=True)  15.7 us
    pallas_call x1, Pallas kernels, enter(): pl.pallas_call(enter_body, in_specs=[hbm] * 4, out_specs=[hbm, hbm], out_...  4.61 us
  transfers between devices with their start and end apart: 1, of which 0 were waited for; matrix products, arithmetic and copies ran while one was open for 0% of the time, Pallas kernels for 54%

profile of v7, /device:TPU:1, one launch (start us, length us, event | category | flops | bytes accessed | tf_op | source)
XLA Modules:
  0.0 123.8 jit_solution(4003194952835681681)
XLA Ops:
  0.0 4.6 %enter.1 = (bf16[2,1024,128]{2,1,0:T(8,128)(2,1)}, bf16[256,2048]{1,0:T(8,128)(2,1)}) custom-call(bf16[2,128,2048]{2,1,0:T(8,128)(2,1)} %tokens.1, f32[1,2048]{1,0:T(1,128)} %bitcast.10, bf16[2048,1024]{1,0:T(8,128)(2,1)} %weight.2, bf16[256,256]{1,0:T(8,128)(2,1)} %constant.35.clone.table), custom_call_target="tpu_custom_call" | custom-call | tf_op jit(solution)/shard_map/enter/pallas_call | solution.py:123
  4.6 15.7 %all-to-all-start = ((bf16[256,8,128]{2,1,0:T(8,128)(2,1)}), bf16[256,8,128]{2,1,0:T(8,128)(2,1)S(1)}, u32[]{:S(2)}, u32[]{:S(2)}) async-start(bf16[256,8,128]{2,1,0:T(8,128)(2,1)} %bitcast.9), calls=%async_computation | async-start | bytes 1048576 | tf_op jit(solution)/shard_map/all_to_all | solution.py:323
  20.3 0.0 copy-start.2
  20.3 0.0 copy-start.3
  20.3 0.0 copy-start.5
  20.3 66.3 %gate.1 = (bf16[256,2048]{1,0:T(8,128)(2,1)S(1)}, bf16[1024,512]{1,0:T(8,128)(2,1)S(1)}, bf16[1024,512]{1,0:T(8,128)(2,1)}, bf16[1024,512]{1,0:T(8,128)(2,1)}) custom-call(bf16[256,2048]{1,0:T(8,128)(2,1)} %get-tuple-element.19.normed, bf16[2048,2048]{1,0:T(8,128)(2,1)} %weight.3, bf16[1024,2048]{1,0:T(8,128)(2,1)} %later.3), custom_call_target="tpu_custom_call" | custom-call | flops 2147483648 | bytes 8388608 | tf_op jit(solution)/shard_map/gate/pallas_call | solution.py:256
  86.7 0.0 copy-start.4
  86.7 0.0 all-to-all-done
  86.7 0.0 copy-start
  86.7 0.0 copy-start.1
  86.7 0.0 copy-done.2
  86.7 0.0 copy-done.3
  86.7 0.0 copy-done.5
  86.7 1.4 %length.1 = (bf16[2048,128]{1,0:T(8,128)(2,1)S(1)}, bf16[1024,512]{1,0:T(8,128)(2,1)S(1)}) custom-call(f32[1]{0:T(128)} %bitcast.lone, bf16[2048,128]{1,0:T(8,128)(2,1)S(1)} %bitcast.6, bf16[512,256]{1,0:T(8,128)(2,1)S(1)} %copy-done.3, f32[2,256,128]{2,1,0:T(8,128)S(1)} %copy-done.2, bf16[128,256]{1,0:T(8,128)(2,1)S(1)} %copy-done.5, bf16[1024,2048]{1,0:T(8,128)(2,1)} %later.3), custom_call_target="tpu_custom_call" | custom-call | tf_op jit(solution)/shard_map/length/pallas_call | solution.py:201
  88.1 33.5 %all_to_all.10 = bf16[256,8,128]{2,1,0:T(8,128)(2,1)S(1)} all-to-all(bf16[256,8,128]{2,1,0:T(8,128)(2,1)S(1)} %bitcast.8), channel_id=1, replica_groups=mesh['row'=32,'col'=8] {'row','col'}, dimensions={0} | all-to-all | bytes 1048576 | tf_op jit(solution)/shard_map/all_to_all | solution.py:323
  121.6 0.0 copy-done.4
  121.6 0.0 copy-done
  121.6 0.0 copy-done.1
  121.6 2.2 %leave.1 = bf16[2,128,2048]{2,1,0:T(8,128)(2,1)} custom-call(bf16[2048,128]{1,0:T(8,128)(2,1)S(1)} %bitcast.7, bf16[256,256]{1,0:T(8,128)(2,1)S(1)} %copy-done.4, bf16[256,2048]{1,0:T(8,128)(2,1)S(1)} %get-tuple-element.26.gates, bf16[1024,512]{1,0:T(8,128)(2,1)S(1)} %get-tuple-element.27.refs_0_, bf16[1024,512]{1,0:T(8,128)(2,1)S(1)} %get-tuple-element.28.refs_1_, ...), custom_call_target="tpu_custom_call" | custom-call | tf_op jit(solution)/shard_map/leave/pallas_call | solution.py:303
Async XLA Ops:
  4.6 82.1 %all-to-all-start = ((bf16[256,8,128]{2,1,0:T(8,128)(2,1)}), bf16[256,8,128]{2,1,0:T(8,128)(2,1)S(1)}, u32[]{:S(2)}, u32[]{:S(2)}) async-start(bf16[256,8,128]{2,1,0:T(8,128)(2,1)} %bitcast.9), calls=%async_computation | async-start | bytes 1048576 | tf_op jit(solution)/shard_map/all_to_all | solution.py:323
  20.3 66.4 %copy-start.2 = (f32[2,256,128]{2,1,0:T(8,128)S(1)}, f32[2,256,128]{2,1,0:T(8,128)}, u32[]{:S(2)}) copy-start(f32[2,256,128]{2,1,0:T(8,128)} %constant.37.clone.twist) | copy-start | bytes 786436
  20.3 66.4 %copy-start.3 = (bf16[512,256]{1,0:T(8,128)(2,1)S(1)}, bf16[512,256]{1,0:T(8,128)(2,1)}, u32[]{:S(2)}) copy-start(bf16[512,256]{1,0:T(8,128)(2,1)} %constant.36.clone.first) | copy-start | bytes 786436
  20.3 66.4 %copy-start.5 = (bf16[128,256]{1,0:T(8,128)(2,1)S(1)}, bf16[128,256]{1,0:T(8,128)(2,1)}, u32[]{:S(2)}) copy-start(bf16[128,256]{1,0:T(8,128)(2,1)} %constant.38.clone.second) | copy-start | bytes 196612
  86.7 34.9 %copy-start.4 = (bf16[256,256]{1,0:T(8,128)(2,1)S(1)}, bf16[256,256]{1,0:T(8,128)(2,1)}, u32[]{:S(2)}) copy-start(bf16[256,256]{1,0:T(8,128)(2,1)} %constant.39.clone.order) | copy-start | bytes 393220
  86.7 34.9 %copy-start = (bf16[1024,512]{1,0:T(8,128)(2,1)S(1)}, bf16[1024,512]{1,0:T(8,128)(2,1)}, u32[]{:S(2)}) copy-start(bf16[1024,512]{1,0:T(8,128)(2,1)} %get-tuple-element.29.refs_2_) | copy-start | bytes 3145732
  86.7 34.9 %copy-start.1 = (bf16[1024,512]{1,0:T(8,128)(2,1)S(1)}, bf16[1024,512]{1,0:T(8,128)(2,1)}, u32[]{:S(2)}) copy-start(bf16[1024,512]{1,0:T(8,128)(2,1)} %get-tuple-element.30.refs_3_) | copy-start | bytes 3145732

commit v8 on v7

--- a/solution.py
+++ b/solution.py
@@ -231,22 +231,31 @@
 
 
 def gate_body(normed, weight, later, out, kept, *refs):
-    loads = [pltpu.make_async_copy(later.at[:, :PARTS], kept, refs[-1].at[0])]
+    cut_off, (passing, sems) = refs[:-2], refs[-2:]
+    own = pltpu.make_async_copy(later.at[:, :PARTS], kept, sems.at[0])
+    loads, stores = [], []
     for c, cut in enumerate(LATE):
-        loads.append(pltpu.make_async_copy(later.at[:, cut], refs[c], refs[-1].at[1 + c]))
+        loads.append(pltpu.make_async_copy(later.at[:, cut], passing.at[c], sems.at[1 + c]))
+        stores.append(pltpu.make_async_copy(passing.at[c], cut_off[c], sems.at[LEAVE + c]))
 
     @pl.when(pl.program_id(0) == 0)
     def _():
-        for load in loads:
+        for load in (*loads, own):
             load.start()
 
     logits = jnp.dot(normed[...], weight[...], preferred_element_type=F32)
     out[...] = jax.nn.sigmoid(logits).astype(BF16)
 
+    @pl.when(pl.program_id(0) == pl.num_programs(0) // 2)
+    def _():
+        for load, store in zip(loads, stores):
+            load.wait()
+            store.start()
+
     @pl.when(pl.program_id(0) == pl.num_programs(0) - 1)
     def _():
-        for load in loads:
-            load.wait()
+        for copy in (own, *stores):
+            copy.wait()
 
 
 def gate(normed, weight, later):
@@ -268,7 +277,10 @@
         + [hbm] * len(LATE),
         out_shape=[pltpu.VMEM((SEQS * BLOCK, D), BF16), pltpu.VMEM((FW, PARTS), BF16)]
         + [pltpu.HBM((FW, PARTS), BF16)] * len(LATE),
-        scratch_shapes=[pltpu.SemaphoreType.DMA((1 + len(LATE),))],
+        scratch_shapes=[
+            pltpu.VMEM((len(LATE), FW, PARTS), BF16),
+            pltpu.SemaphoreType.DMA((2 * LEAVE,)),
+        ],
         cost_estimate=pl.CostEstimate(
             flops=2 * SEQS * BLOCK * D * D, transcendentals=SEQS * BLOCK * D, bytes_accessed=2 * D * D
         ),

time: 124 us -> 69.9 us (0.56)
  Pallas kernels: 74.5 us -> 17.3 us
  waiting for transfers between devices: 0.01 us -> 10.7 us
  blocking collectives: 33.5 us -> 25.9 us
    pallas_call x1, Pallas kernels: 66.3 us -> 9.12 us  [gate(): pl.pallas_call(gate_body, grid=(steps,), in_specs=[pl.BlockSpec((SEQS * B...]
    all_to_all x1, waiting for transfers between devices: 0.01 us -> 10.7 us  [exchange(): lax.all_to_all(x.reshape(DEVICES, ROWS, BLOCK), AXES, 0, 0, tiled=True)]
    all_to_all x1, blocking collectives: 33.5 us -> 25.9 us  [exchange(): lax.all_to_all(x.reshape(DEVICES, ROWS, BLOCK), AXES, 0, 0, tiled=True)]
  transfers between devices with their start and end apart: 1 -> 1, of which waited for: 0 -> 1; matrix products, arithmetic and copies ran while one was open for 0% -> 0% of each run, Pallas kernels for 54% -> 13%
where the time goes in v8:
time: 69.9 us; the launch traced here: 69.7 us
  blocking collectives  25.9 us (37%)
  Pallas kernels  17.3 us (25%)
  starting transfers between devices  15.7 us (22%)
  waiting for transfers between devices  10.7 us (15%)
    all_to_all x1, blocking collectives, exchange(): lax.all_to_all(x.reshape(DEVICES, ROWS, BLOCK), AXES, 0, 0, tiled=True)  25.9 us
    all_to_all x1, starting transfers between devices, exchange(): lax.all_to_all(x.reshape(DEVICES, ROWS, BLOCK), AXES, 0, 0, tiled=True)  15.7 us
    all_to_all x1, waiting for transfers between devices, exchange(): lax.all_to_all(x.reshape(DEVICES, ROWS, BLOCK), AXES, 0, 0, tiled=True)  10.7 us
    pallas_call x1, Pallas kernels, gate(): pl.pallas_call(gate_body, grid=(steps,), in_specs=[pl.BlockSpec((SEQS * B...  9.12 us
    pallas_call x1, Pallas kernels, enter(): pl.pallas_call(enter_body, in_specs=[hbm] * 4, out_specs=[hbm, hbm], out_...  4.61 us
    pallas_call x1, Pallas kernels, leave(): pl.pallas_call(leave_body, in_specs=[vmem] * (3 + len(parts)), out_specs=...  2.17 us
  transfers between devices with their start and end apart: 1, of which 1 were waited for; matrix products, arithmetic and copies ran while one was open for 0% of the time, Pallas kernels for 13%

profile of v8, /device:TPU:1, one launch (start us, length us, event | category | flops | bytes accessed | tf_op | source)
XLA Modules:
  0.0 69.7 jit_solution(3187725481033275287)
XLA Ops:
  0.0 4.6 %enter.1 = (bf16[2,1024,128]{2,1,0:T(8,128)(2,1)}, bf16[256,2048]{1,0:T(8,128)(2,1)}) custom-call(bf16[2,128,2048]{2,1,0:T(8,128)(2,1)} %tokens.1, f32[1,2048]{1,0:T(1,128)} %bitcast.10, bf16[2048,1024]{1,0:T(8,128)(2,1)} %weight.2, bf16[256,256]{1,0:T(8,128)(2,1)} %constant.35.clone.table), custom_call_target="tpu_custom_call" | custom-call | tf_op jit(solution)/shard_map/enter/pallas_call | solution.py:123
  4.6 15.7 %all-to-all-start = ((bf16[256,8,128]{2,1,0:T(8,128)(2,1)}), bf16[256,8,128]{2,1,0:T(8,128)(2,1)S(1)}, u32[]{:S(2)}, u32[]{:S(2)}) async-start(bf16[256,8,128]{2,1,0:T(8,128)(2,1)} %bitcast.9), calls=%async_computation | async-start | bytes 1048576 | tf_op jit(solution)/shard_map/all_to_all | solution.py:335
  20.3 0.0 copy-start.2
  20.3 0.0 copy-start.3
  20.3 0.0 copy-start.5
  20.3 9.1 %gate.1 = (bf16[256,2048]{1,0:T(8,128)(2,1)S(1)}, bf16[1024,512]{1,0:T(8,128)(2,1)S(1)}, bf16[1024,512]{1,0:T(8,128)(2,1)}, bf16[1024,512]{1,0:T(8,128)(2,1)}) custom-call(bf16[256,2048]{1,0:T(8,128)(2,1)} %get-tuple-element.19.normed, bf16[2048,2048]{1,0:T(8,128)(2,1)} %weight.3, bf16[1024,2048]{1,0:T(8,128)(2,1)} %later.3), custom_call_target="tpu_custom_call" | custom-call | flops 2147483648 | bytes 8388608 | tf_op jit(solution)/shard_map/gate/pallas_call | solution.py:265
  29.5 0.0 copy-start.4
  29.5 10.7 %all-to-all-done = bf16[256,8,128]{2,1,0:T(8,128)(2,1)S(1)} async-done(((bf16[256,8,128]{2,1,0:T(8,128)(2,1)}), bf16[256,8,128]{2,1,0:T(8,128)(2,1)S(1)}, u32[]{:S(2)}, u32[]{:S(2)}) %all-to-all-start) | async-done | bytes 524320 | tf_op jit(solution)/shard_map/all_to_all | solution.py:335
  40.2 0.0 copy-start
  40.2 0.0 copy-start.1
  40.2 0.0 copy-done.2
  40.2 0.0 copy-done.3
  40.2 0.0 copy-done.5
  40.2 1.4 %length.1 = (bf16[2048,128]{1,0:T(8,128)(2,1)S(1)}, bf16[1024,512]{1,0:T(8,128)(2,1)S(1)}) custom-call(f32[1]{0:T(128)} %bitcast.lone, bf16[2048,128]{1,0:T(8,128)(2,1)S(1)} %bitcast.6, bf16[512,256]{1,0:T(8,128)(2,1)S(1)} %copy-done.3, f32[2,256,128]{2,1,0:T(8,128)S(1)} %copy-done.2, bf16[128,256]{1,0:T(8,128)(2,1)S(1)} %copy-done.5, bf16[1024,2048]{1,0:T(8,128)(2,1)} %later.3), custom_call_target="tpu_custom_call" | custom-call | tf_op jit(solution)/shard_map/length/pallas_call | solution.py:201
  41.6 25.9 %all_to_all.10 = bf16[256,8,128]{2,1,0:T(8,128)(2,1)S(1)} all-to-all(bf16[256,8,128]{2,1,0:T(8,128)(2,1)S(1)} %bitcast.8), channel_id=1, replica_groups=mesh['row'=32,'col'=8] {'row','col'}, dimensions={0} | all-to-all | bytes 1048576 | tf_op jit(solution)/shard_map/all_to_all | solution.py:335
  67.5 0.0 copy-done.4
  67.5 0.0 copy-done
  67.5 0.0 copy-done.1
  67.5 2.2 %leave.1 = bf16[2,128,2048]{2,1,0:T(8,128)(2,1)} custom-call(bf16[2048,128]{1,0:T(8,128)(2,1)S(1)} %bitcast.7, bf16[256,256]{1,0:T(8,128)(2,1)S(1)} %copy-done.4, bf16[256,2048]{1,0:T(8,128)(2,1)S(1)} %get-tuple-element.26.gates, bf16[1024,512]{1,0:T(8,128)(2,1)S(1)} %get-tuple-element.27.refs_0_, bf16[1024,512]{1,0:T(8,128)(2,1)S(1)} %get-tuple-element.28.refs_1_, ...), custom_call_target="tpu_custom_call" | custom-call | tf_op jit(solution)/shard_map/leave/pallas_call | solution.py:315
Async XLA Ops:
  4.6 35.6 %all-to-all-start = ((bf16[256,8,128]{2,1,0:T(8,128)(2,1)}), bf16[256,8,128]{2,1,0:T(8,128)(2,1)S(1)}, u32[]{:S(2)}, u32[]{:S(2)}) async-start(bf16[256,8,128]{2,1,0:T(8,128)(2,1)} %bitcast.9), calls=%async_computation | async-start | bytes 1048576 | tf_op jit(solution)/shard_map/all_to_all | solution.py:335
  20.3 19.9 %copy-start.2 = (f32[2,256,128]{2,1,0:T(8,128)S(1)}, f32[2,256,128]{2,1,0:T(8,128)}, u32[]{:S(2)}) copy-start(f32[2,256,128]{2,1,0:T(8,128)} %constant.37.clone.twist) | copy-start | bytes 786436
  20.3 19.9 %copy-start.3 = (bf16[512,256]{1,0:T(8,128)(2,1)S(1)}, bf16[512,256]{1,0:T(8,128)(2,1)}, u32[]{:S(2)}) copy-start(bf16[512,256]{1,0:T(8,128)(2,1)} %constant.36.clone.first) | copy-start | bytes 786436
  20.3 19.9 %copy-start.5 = (bf16[128,256]{1,0:T(8,128)(2,1)S(1)}, bf16[128,256]{1,0:T(8,128)(2,1)}, u32[]{:S(2)}) copy-start(bf16[128,256]{1,0:T(8,128)(2,1)} %constant.38.clone.second) | copy-start | bytes 196612
  29.5 38.0 %copy-start.4 = (bf16[256,256]{1,0:T(8,128)(2,1)S(1)}, bf16[256,256]{1,0:T(8,128)(2,1)}, u32[]{:S(2)}) copy-start(bf16[256,256]{1,0:T(8,128)(2,1)} %constant.39.clone.order) | copy-start | bytes 393220
  40.2 27.3 %copy-start = (bf16[1024,512]{1,0:T(8,128)(2,1)S(1)}, bf16[1024,512]{1,0:T(8,128)(2,1)}, u32[]{:S(2)}) copy-start(bf16[1024,512]{1,0:T(8,128)(2,1)} %get-tuple-element.29.refs_2_) | copy-start | bytes 3145732
  40.2 27.3 %copy-start.1 = (bf16[1024,512]{1,0:T(8,128)(2,1)S(1)}, bf16[1024,512]{1,0:T(8,128)(2,1)}, u32[]{:S(2)}) copy-start(bf16[1024,512]{1,0:T(8,128)(2,1)} %get-tuple-element.30.refs_3_) | copy-start | bytes 3145732
